TPU v7x, 512 devices: a whole 4x4x16 slice. The times are simulated.
512 devices in a mesh: fs: 16 (over y, x), tp: 32 (over z, core).
Axes of the slice: x: 4, y: 4, z: 16, core: 2. Of those that a mesh axis runs over, the one named last changes fastest.
Arguments:
- tokens: bfloat16 [65536, 2048], P(('fs', 'tp')), may hold values from -6 to 6
- gain: float32 [2048], P('fs'), may hold values from 0.1 to 1.9
- ex_gate: float32 [32, 256, 2048], P('tp', None, 'fs'), may hold values from -0.125 to 0.125
- ex_up: float32 [32, 256, 2048], P('tp', None, 'fs'), may hold values from -0.125 to 0.125
- ex_down: float32 [32, 256, 2048], P('tp', None, 'fs'), may hold values from -0.375 to 0.375
- sh_gate: float32 [512, 2048], P('tp', 'fs'), may hold values from -0.125 to 0.125
- sh_up: float32 [512, 2048], P('tp', 'fs'), may hold values from -0.125 to 0.125
- sh_down: float32 [512, 2048], P('tp', 'fs'), may hold values from -0.25 to 0.25
- routes: int32 [65536, 4], P(('fs', 'tp')), may hold values from 0 to 31, all different within a row; in each aligned block of 128 rows (0 to 127, 128 to 255, ...) at most 18 rows name the same one
- route_weight: float32 [65536, 4], P(('fs', 'tp')), may hold values from 0.1 to 1
Outputs:
- mixed: bfloat16 [65536, 2048], P(('fs', 'tp'))
- expert_gate: bfloat16 [32, 256, 2048], P('tp')
- expert_up: bfloat16 [32, 256, 2048], P('tp')
- expert_down: bfloat16 [32, 256, 2048], P('tp')
- shared_gate: bfloat16 [512, 2048], P('tp')
- shared_up: bfloat16 [512, 2048], P('tp')
- shared_down: bfloat16 [512, 2048], P('tp')
Inputs may be any that keep to these rules, and one draw needn't show every extreme that they name: `routes`: each row names 4 different experts. Among the rows of one device no expert is named by more than 18 rows, and in every draw some expert is named by exactly 18 rows of some device.
All inputs are finite; a program needn't handle non-finite values.
Results may differ from a plain program's by a relative error of at most 0.0085.
Values may be sent and summed in bfloat16 or wider, within the bound.
No kernel may reach another device: no remote copies, remote signals or barrier semaphores. Data moves between devices by JAX's collectives and lax.ppermute only.
A program may use at most 64 MiB of HBM per device.

v0:
```python
import jax
import jax.numpy as jnp
from jax import lax
from jax.sharding import Mesh
from jax.sharding import PartitionSpec as P

TP = ("tp_0", "tp_1")
FS_TP = ("fs", "tp_0", "tp_1")


EPS = 1e-06
ROUTED_SCALE = 2.5
CONTRACT = (((1,), (1,)), ((), ()))


def in_one_piece(arrays, axis, dim, along):
    ends, at = ([], 0)
    for a in arrays[:-1]:
        at += a.shape[along]
        ends.append(at)
    both = jnp.concatenate(arrays, axis=along)
    return tuple(jnp.split(lax.all_gather(both, axis, axis=dim, tiled=True), ends, axis=along))


def in_blocks(array, dim, devices):
    before, after = (array.shape[:dim], array.shape[dim + 1 :])
    return jnp.moveaxis(array.reshape(*before, devices, -1, *after), dim, 0)


def laid_out(tiles, dim):
    tiles = jnp.moveaxis(tiles, 0, dim)
    lengths = tiles.shape
    return tiles.reshape(*lengths[:dim], lengths[dim] * lengths[dim + 1], *lengths[dim + 2 :])


def turned_blocks(tiles, axes, turns):
    lengths = [lax.axis_size(a) for a in axes]
    tiles = tiles.reshape(*lengths, *tiles.shape[1:])
    for k in turns:
        tiles = lax.all_to_all(tiles, axes[k], split_axis=k, concat_axis=k, tiled=True)
    return tiles.reshape(-1, *tiles.shape[len(axes) :])


def two_step_exchange(array, groups, turns, split_dim, concat_dim):
    devices = lax.axis_size(groups[0]) * lax.axis_size(groups[1])
    tiles = in_blocks(array, split_dim, devices)
    return laid_out(turned_blocks(tiles, groups, turns), concat_dim)


def against(row_block, weight):
    return lax.dot_general(row_block, weight, CONTRACT, preferred_element_type=jnp.float32)


def hidden_of(row_block, w_gate, w_up):
    return (jax.nn.silu(against(row_block, w_gate)) * against(row_block, w_up)).astype(jnp.bfloat16)


def expert_apply(row_block, w_gate, w_up, w_down):
    return jnp.dot(hidden_of(row_block, w_gate, w_up), w_down, preferred_element_type=jnp.float32)


def slot_numbers(expert_ids, experts, capacity):
    flat_ids = expert_ids.reshape(-1)
    onehot = (flat_ids[:, None] == jnp.arange(experts, dtype=jnp.int32)[None, :]).astype(jnp.int32)
    before = jnp.cumsum(onehot, axis=0) - onehot
    ranking = jnp.sum(before * onehot, axis=1)
    return flat_ids * capacity + ranking


def local(tokens, gain, ex_gate, ex_up, ex_down, sh_gate, sh_up, sh_down, routes, route_weight):
    scale = gain[None, :]
    fold_gate = (ex_gate * scale[None]).astype(jnp.bfloat16)
    fold_up = (ex_up * scale[None]).astype(jnp.bfloat16)
    fold_down = ex_down.astype(jnp.bfloat16)
    fold_sgate = (sh_gate * scale).astype(jnp.bfloat16)[None]
    fold_sup = (sh_up * scale).astype(jnp.bfloat16)[None]
    fold_sdown = sh_down.astype(jnp.bfloat16)[None]
    tok_rows = tokens.shape[0]
    width = tokens.shape[1]
    top = routes.shape[1]
    experts = lax.axis_size(TP)
    capacity = tok_rows * top * 9 // (8 * experts)
    values = tokens.astype(jnp.float32)
    normed = (values * lax.rsqrt(jnp.mean(values * values, axis=1, keepdims=True) + EPS)).astype(
        jnp.bfloat16
    )
    weights = route_weight / jnp.sum(route_weight, axis=1, keepdims=True) * ROUTED_SCALE
    slots = slot_numbers(routes, experts, capacity)
    spots = jnp.arange(experts * capacity, dtype=jnp.int32)
    placing = (spots[:, None] == slots[None, :]).astype(jnp.int32)
    placing = jnp.sum(placing.reshape(experts * capacity, tok_rows, top), axis=2).astype(
        jnp.bfloat16
    )
    outgoing = jnp.dot(placing, normed, preferred_element_type=jnp.float32).astype(jnp.bfloat16)
    outgoing = outgoing.reshape(experts, capacity, width)
    whole = in_one_piece(
        (fold_gate, fold_up, fold_down, fold_sgate, fold_sup, fold_sdown), "fs", 2, 1
    )
    exp_gate, exp_up, exp_down = (whole[0], whole[1], whole[2])
    shr_gate, shr_up, shr_down = (whole[3][0], whole[4][0], whole[5][0])
    arrived = lax.all_to_all(outgoing, TP, split_axis=0, concat_axis=0, tiled=True)
    sources = arrived.shape[0]
    count = arrived.shape[1]
    flat_rows = arrived.reshape(sources * count, width)
    result = expert_apply(flat_rows, exp_gate[0], exp_up[0], exp_down[0]).astype(jnp.bfloat16)
    answered = result.reshape(sources, count, width)
    returned = two_step_exchange(answered, ("tp_0", "tp_1"), (1, 0), 0, 0).reshape(
        experts * capacity, width
    )
    picked = returned[slots].reshape(tok_rows, top, width)
    routed = jnp.sum(weights[:, :, None] * picked.astype(jnp.float32), axis=1)
    pieces = in_one_piece((shr_gate, shr_up, shr_down), TP, 0, 1)
    shared = expert_apply(normed, pieces[0], pieces[1], pieces[2])
    mixed = (shared + routed).astype(jnp.bfloat16)
    return (mixed, exp_gate, exp_up, exp_down, shr_gate, shr_up, shr_down)


def solution(mesh):
    split = Mesh(mesh.devices.reshape(mesh.shape["fs"], 16, 2), ("fs", "tp_0", "tp_1"))
    in_specs = (
        P(FS_TP, None),
        P("fs"),
        P(TP, None, "fs"),
        P(TP, None, "fs"),
        P(TP, None, "fs"),
        P(TP, "fs"),
        P(TP, "fs"),
        P(TP, "fs"),
        P(FS_TP, None),
        P(FS_TP, None),
    )
    out_specs = (
        P(FS_TP, None),
        P(TP, None, None),
        P(TP, None, None),
        P(TP, None, None),
        P(TP, None),
        P(TP, None),
        P(TP, None),
    )
    return jax.shard_map(local, mesh=split, in_specs=in_specs, out_specs=out_specs, check_vma=False)
```

profile of v0, /device:TPU:46, one launch (start us, length us, event | category | flops | bytes accessed | tf_op | source)
XLA Modules:
  0.0 365.8 jit_solution(3601061499038751785)
XLA Ops:
  7.2 0.0 all-gather.3.cloned.1.call-start
  7.2 1.0 fusion.35
  8.2 0.9 fusion.36
  9.1 0.9 convert_dynamic-update-slice_fusion
  10.0 0.7 constant_dynamic-update-slice_fusion.2
  10.8 0.7 constant_dynamic-update-slice_fusion.1
  11.5 0.7 constant_dynamic-update-slice_fusion
  12.2 0.7 copy-done.4
  12.8 0.0 all-gather.3.cloned.1.call-update
  12.9 0.8 copy.33
  13.7 0.1 eq.44
  13.8 0.1 eq.40
  13.9 1.2 reduce-window.6
  15.1 0.2 slice_reduce_fusion
  15.3 0.1 fusion.39
  15.4 0.1 reduce_sum.52
  15.6 1.2 fusion.15
  16.8 0.1 copy.37
  16.9 0.2 convert_reduce_fusion
  17.0 0.8 convolution_convert_fusion.1
  17.9 2.4 reshape.101
  20.3 15.4 %all-to-all-start = ((bf16[32,18,2048]{2,1,0:T(8,128)(2,1)}), bf16[32,18,2048]{2,1,0:T(8,128)(2,1)S(1)}, u32[]{:S(2)}, u32[]{:S(2)}) async-start(bf16[32,18,2048]{2,1,0:T(8,128)(2,1)} %reshape.101), calls=%async_computation | async-start | bytes 6291456 | tf_op jit(solution)/shard_map/all_to_all | solution.py:101
  35.7 0.0 all-gather.5.cloned.1.call-start
  35.7 47.7 %all-gather.3.cloned.1.call-done = bf16[1,816,2048]{2,1,0:T(8,128)(2,1)} async-done(((bf16[1,816,128]{2,1,0:T(8,128)(2,1)}), bf16[1,816,2048]{2,1,0:T(8,128)(2,1)}) %all-gather.3.cloned.1.call-update) | async-done | bytes 3342352 | tf_op jit(solution)/shard_map/all_gather | solution.py:22
  83.5 0.9 slice_bitcast_fusion.2
  84.4 0.7 pad_maximum_fusion
  85.1 0.0 all-gather.5.cloned.1.call-update
  85.2 3.6 fusion.50
  88.8 109.1 %all-to-all-done = bf16[32,18,2048]{2,1,0:T(8,128)(2,1)S(1)} async-done(((bf16[32,18,2048]{2,1,0:T(8,128)(2,1)}), bf16[32,18,2048]{2,1,0:T(8,128)(2,1)S(1)}, u32[]{:S(2)}, u32[]{:S(2)}) %all-to-all-start) | async-done | bytes 2359328 | tf_op jit(solution)/shard_map/all_to_all | solution.py:101
  197.9 2.3 reshape.102
  200.2 3.8 %fusion.20 = f32[576,256]{1,0:T(8,128)} fusion(bf16[576,2048]{1,0:T(8,128)(2,1)} %reshape.102, bf16[1,256,2048]{2,1,0:T(8,128)(2,1)} %get-tuple-element.10), kind=kOutput, calls=%fused_computation.23 | convolution fusion | flops 603979776 | bytes 3997696 | tf_op jit(solution)/shard_map/dot_general | solution.py:51
  204.0 5.4 %convolution_convert_fusion = bf16[576,2048]{1,0:T(8,128)(2,1)} fusion(bf16[576,2048]{1,0:T(8,128)(2,1)S(1)} %copy-done, bf16[1,256,2048]{2,1,0:T(8,128)(2,1)S(1)} %copy-done.3, bf16[1,256,2048]{2,1,0:T(8,128)(2,1)} %get-tuple-element.12, f32[576,256]{1,0:T(8,128)} %fusion.20), kind=kOutput, calls=%fused_computation.2 | convolution fusion | flops 1210023936 | bytes 7405568 | tf_op jit(solution)/shard_map/dot_general | solution.py:59
  209.4 2.7 reshape_reshape_reshape.6
  212.1 1.3 copy.38
  213.4 5.6 %all_to_all.15 = bf16[16,2,1,18,2048]{4,0,3,2,1:T(8,128)(2,1)S(1)} all-to-all(bf16[16,2,1,18,2048]{4,0,3,2,1:T(8,128)(2,1)S(1)} %copy.38), channel_id=1, replica_groups=mesh['fs'=16,'tp_0'=16,'tp_1'=2] {'tp_1'}, dimensions={1} | all-to-all | bytes 4718592 | tf_op jit(solution)/shard_map/all_to_all | solution.py:40
  219.1 3.8 %copy.39 = bf16[16,2,1,18,2048]{4,1,3,2,0:T(2,128)(2,1)} copy(bf16[16,2,1,18,2048]{4,0,3,2,1:T(8,128)(2,1)S(1)} %all_to_all.15) | data formatting | bytes 4718592 | tf_op jit(solution)/shard_map/all_to_all | solution.py:40
  222.9 5.1 %all-to-all-start.2 = ((bf16[16,2,1,18,2048]{4,1,3,2,0:T(2,128)(2,1)}), bf16[16,2,1,18,2048]{4,1,3,2,0:T(2,128)(2,1)S(1)}, u32[]{:S(2)}, u32[]{:S(2)}) async-start(bf16[16,2,1,18,2048]{4,1,3,2,0:T(2,128)(2,1)} %copy.39), calls=%async_computation.2 | async-start | bytes 4718592 | tf_op jit(solution)/shard_map/all_to_all | solution.py:40
  228.1 0.1 mul.109
  228.2 0.1 copy.32
  228.3 104.7 %all-to-all-done.2 = bf16[16,2,1,18,2048]{4,1,3,2,0:T(2,128)(2,1)S(1)} async-done(((bf16[16,2,1,18,2048]{4,1,3,2,0:T(2,128)(2,1)}), bf16[16,2,1,18,2048]{4,1,3,2,0:T(2,128)(2,1)S(1)}, u32[]{:S(2)}, u32[]{:S(2)}) %all-to-all-start.2) | async-done | bytes 2359328 | tf_op jit(solution)/shard_map/all_to_all | solution.py:40
  333.0 2.9 copy.40
  335.9 2.9 reshape_reshape_reshape.7
  338.8 3.3 gather_fusion
  342.1 4.8 %reshape.103 = f32[128,4,2048]{2,1,0:T(4,128)} reshape(bf16[512,2048]{1,0:T(8,128)(2,1)} %gather_fusion) | data formatting | bytes 6291456 | tf_op jit(solution)/shard_map/convert_element_type | solution.py:111
  346.8 5.4 %multiply_reduce_fusion = f32[128,2048]{1,0:T(8,128)S(1)} fusion(f32[128,4,2048]{2,1,0:T(4,128)} %reshape.103, f32[128,4]{1,0:T(8,128)S(1)} %copy.32), kind=kLoop, calls=%fused_computation.1 | loop fusion | flops 1835008 | bytes 5244928 | tf_op jit(solution)/shard_map/reduce_sum | solution.py:111
  352.3 0.0 all-gather.5.cloned.1.call-done
  352.3 2.4 fusion.4
  354.7 4.3 %fusion = bf16[128,2048]{1,0:T(8,128)(2,1)} fusion(f32[128,2048]{1,0:T(8,128)S(1)} %multiply_reduce_fusion, bf16[512,6144]{1,0:T(8,128)(2,1)} %all-gather.5.cloned.1.call-done, f32[128,512]{1,0:T(8,128)S(1)} %fusion.4, bf16[128,2048]{1,0:T(8,128)(2,1)S(1)} %copy-done.2, f32[128]{0:T(128)S(1)} %add_rsqrt_fusion), kind=kOutput, calls=%fused_computation.5 | convolution fusion | flops 538574848 | bytes 6554112 | tf_op jit(solution)/shard_map/dot_general | solution.py:59
  (26 shorter events, 0.2 us)
Async XLA Ops:
  7.2 9.9 %copy-start.1 = (bf16[128,2048]{1,0:T(8,128)(2,1)S(1)}, bf16[128,2048]{1,0:T(8,128)(2,1)}, u32[]{:S(2)}) copy-start(bf16[128,2048]{1,0:T(8,128)(2,1)} %param.10) | copy-start | bytes 1572868
  7.2 76.3 %all-gather.3.cloned.1.call-start = ((), (), s32[]{:S(2)}) async-start(), calls=%async_computation.3 | async-start | bytes 3551232 | tf_op jit(solution)/shard_map/all_gather | solution.py:22
  12.2 0.7 copy-start.4
  20.3 177.6 %all-to-all-start = ((bf16[32,18,2048]{2,1,0:T(8,128)(2,1)}), bf16[32,18,2048]{2,1,0:T(8,128)(2,1)S(1)}, u32[]{:S(2)}, u32[]{:S(2)}) async-start(bf16[32,18,2048]{2,1,0:T(8,128)(2,1)} %reshape.101), calls=%async_computation | async-start | bytes 6291456 | tf_op jit(solution)/shard_map/all_to_all | solution.py:101
  35.7 316.6 %all-gather.5.cloned.1.call-start = ((), (), s32[]{:S(2)}) async-start(), calls=%async_computation.4 | async-start | bytes 6488064 | tf_op jit(solution)/shard_map/all_gather | solution.py:22
  84.4 4.4 %copy-start.5 = (bf16[16,2048]{1,0:T(8,128)(2,1)}, bf16[16,2048]{1,0:T(8,128)(2,1)S(1)}, u32[]{:S(2)}) copy-start(bf16[16,2048]{1,0:T(8,128)(2,1)S(1)} %get-tuple-element.7) | copy-start | bytes 196612
  84.4 4.4 %copy-start.6 = (bf16[16,2048]{1,0:T(8,128)(2,1)}, bf16[16,2048]{1,0:T(8,128)(2,1)S(1)}, u32[]{:S(2)}) copy-start(bf16[16,2048]{1,0:T(8,128)(2,1)S(1)} %get-tuple-element.8) | copy-start | bytes 196612
  84.4 4.4 %copy-start.7 = (bf16[16,2048]{1,0:T(8,128)(2,1)}, bf16[16,2048]{1,0:T(8,128)(2,1)S(1)}, u32[]{:S(2)}) copy-start(bf16[16,2048]{1,0:T(8,128)(2,1)S(1)} %get-tuple-element.9) | copy-start | bytes 196612
  200.2 3.8 %copy-start = (bf16[576,2048]{1,0:T(8,128)(2,1)S(1)}, bf16[576,2048]{1,0:T(8,128)(2,1)}, u32[]{:S(2)}) copy-start(bf16[576,2048]{1,0:T(8,128)(2,1)} %reshape.102) | copy-start | bytes 7077892
  200.2 3.8 %copy-start.3 = (bf16[1,256,2048]{2,1,0:T(8,128)(2,1)S(1)}, bf16[1,256,2048]{2,1,0:T(8,128)(2,1)}, u32[]{:S(2)}) copy-start(bf16[1,256,2048]{2,1,0:T(8,128)(2,1)} %get-tuple-element.11) | copy-start | bytes 3145732
  222.9 5.2 %copy-start.8 = (f32[128,4]{0,1:T(4,128)S(1)}, f32[128,4]{0,1:T(4,128)}, u32[]{:S(2)}) copy-start(f32[128,4]{0,1:T(4,128)} %param.19) | copy-start | bytes 6148
  222.9 110.1 %all-to-all-start.2 = ((bf16[16,2,1,18,2048]{4,1,3,2,0:T(2,128)(2,1)}), bf16[16,2,1,18,2048]{4,1,3,2,0:T(2,128)(2,1)S(1)}, u32[]{:S(2)}, u32[]{:S(2)}) async-start(bf16[16,2,1,18,2048]{4,1,3,2,0:T(2,128)(2,1)} %copy.39), calls=%async_computation.2 | async-start | bytes 4718592 | tf_op jit(solution)/shard_map/all_to_all | solution.py:40
  346.8 5.4 %copy-start.2 = (bf16[128,2048]{1,0:T(8,128)(2,1)S(1)}, bf16[128,2048]{1,0:T(8,128)(2,1)}, u32[]{:S(2)}) copy-start(bf16[128,2048]{1,0:T(8,128)(2,1)} %param.10) | copy-start | bytes 1572868
Sparse Core Ops, SparseCore 0:
  13.0 70.4 all-gather.2
  86.2 132.9 all-gather.4
where the time goes:
time: 367 us; the launch traced here: 366 us
  waiting for transfers between devices  262 us (71%)
  local copies, waits for them, and re-layouts  33.3 us (9%)
  starting transfers between devices  20.6 us (6%)
  matrix products  16.7 us (5%)
  between operations  14.2 us (4%)
  other arithmetic  13.8 us (4%)
  blocking collectives  5.63 us (2%)
    all_to_all x1, waiting for transfers between devices, local(): lax.all_to_all(outgoing, TP, split_axis=0, concat_axis=0, tiled=True)  109 us
    all_to_all x1, waiting for transfers between devices, turned_blocks(): lax.all_to_all(tiles, axes[k], split_axis=k, concat_axis=k, tiled=True)  105 us
    all_gather x2, waiting for transfers between devices, in_one_piece(): lax.all_gather(both, axis, axis=dim, tiled=True)  47.8 us
    all_to_all x1, starting transfers between devices, local(): lax.all_to_all(outgoing, TP, split_axis=0, concat_axis=0, tiled=True)  15.4 us
    dot_general x2, matrix products, expert_apply(): jnp.dot(hidden_of(row_block, w_gate, w_up), w_down, preferred_element_typ...  9.69 us
  transfers between devices with their start and end apart: 4, of which 3 were waited for; matrix products, arithmetic and copies ran while one was open for 14% of the time, Pallas kernels for 0%

commit v1 on v0

v1 whole, which is shorter than its diff:
```python
import functools

import jax
import jax.numpy as jnp
from jax import lax
from jax.experimental import pallas as pl
from jax.experimental.pallas import tpu as pltpu
from jax.sharding import Mesh
from jax.sharding import PartitionSpec as P

TP = ("tp_0", "tp_1")
PLANE = ("fs", "tp_1")
FS_TP = ("fs", "tp_0", "tp_1")

EPS = 1e-06
ROUTED_SCALE = 2.5
BF = jnp.bfloat16
F32 = jnp.float32
NT = (((1,), (1,)), ((), ()))

MAIN = 16
EXTRA = 2
QUARTERS = 4


def dot(a, b):
    return jnp.dot(a, b, preferred_element_type=F32)


def dot_nt(a, b):
    return lax.dot_general(a, b, NT, preferred_element_type=F32)


def iota(shape, dim):
    return lax.broadcasted_iota(jnp.int32, shape, dim)


def whole(shape):
    return pl.BlockSpec(shape, lambda: (0,) * len(shape))


def call(body, out, args, flops, name):
    moved = sum(a.size * a.dtype.itemsize for a in args) + sum(o.size * o.dtype.itemsize for o in out)
    return pl.pallas_call(
        body,
        out_shape=out,
        in_specs=[whole(a.shape) for a in args],
        out_specs=[whole(o.shape) for o in out],
        cost_estimate=pl.CostEstimate(flops=flops, bytes_accessed=moved, transcendentals=0),
        name=name,
    )(*args)


def fold_body(gain, eg, eu, ed, sg, su, sd, routed, both):
    scale = gain[...]
    rows = eg.shape[1]
    gate = (eg[0] * scale).astype(BF)
    up = (eu[0] * scale).astype(BF)
    down = ed[0].astype(BF)
    for i, part in enumerate((gate, up, down)):
        routed[i * rows : (i + 1) * rows, :] = part
        both[i * rows : (i + 1) * rows, :] = part
    at = 3 * rows
    few = sg.shape[0]
    for part in (sg[...] * scale, su[...] * scale, sd[...]):
        both[at : at + few, :] = part.astype(BF)
        at += few


def place_body(tokens, routes_t, outgoing, normed_out):
    values = tokens[...].astype(F32)
    mean = jnp.mean(values * values, axis=1, keepdims=True)
    normed = (values * lax.rsqrt(mean + EPS)).astype(BF)
    normed_out[...] = normed
    experts = outgoing.shape[0]
    top, rows = routes_t.shape
    ids = [routes_t[k : k + 1, :] for k in range(top)]
    hot = [(iota((experts, rows), 0) == ids[k]).astype(F32) for k in range(top)]
    named = sum(hot[1:], hot[0])
    earlier = (iota((rows, rows), 0) < iota((rows, rows), 1)).astype(BF)
    before = dot(named.astype(BF), earlier)
    ranks = [jnp.sum(before * h, axis=0, keepdims=True).astype(jnp.int32) for h in hot]
    spot = iota((experts * MAIN, rows), 0)
    main = jnp.zeros((experts * MAIN, rows), F32)
    for k in range(top):
        target = jnp.where(ranks[k] < MAIN, ids[k] * MAIN + ranks[k], -1)
        main = jnp.where(spot == target, 1.0, main)
    main = main.astype(BF)
    few = QUARTERS * EXTRA
    spot = iota((experts * few, rows), 0)
    part = normed.shape[1] // QUARTERS
    extra = jnp.zeros((experts * few, part), F32)
    for q in range(QUARTERS):
        piece = normed[:, q * part : (q + 1) * part]
        rows_q = dot(main, piece).astype(BF)
        outgoing[:, q * MAIN : (q + 1) * MAIN, :] = rows_q.reshape(experts, MAIN, part)
        pick = jnp.zeros((experts * few, rows), F32)
        for k in range(top):
            slot = ids[k] * few + q * EXTRA + ranks[k] - MAIN
            pick = jnp.where(spot == jnp.where(ranks[k] < MAIN, -1, slot), 1.0, pick)
        extra = extra + dot(pick.astype(BF), piece)
    outgoing[:, QUARTERS * MAIN :, :] = extra.reshape(experts, few, part).astype(BF)


def lanes(w, lo, hi, q, per):
    return jnp.concatenate([w[q * per + i, lo:hi, :] for i in range(per)], axis=1)


def expert_body(arrived, w, answered, acc_main, acc_extra, hid_main, hid_extra):
    sources = arrived.shape[0]
    part = arrived.shape[2]
    per = part // w.shape[2]
    width = w.shape[1] // 3
    few = QUARTERS * EXTRA
    tail = arrived[:, QUARTERS * MAIN :, :].astype(F32).reshape(sources * few, part).astype(BF)
    row = iota((sources * EXTRA, sources * few), 0)
    col = iota((sources * EXTRA, sources * few), 1)
    for q in range(QUARTERS):
        both = lanes(w, 0, 2 * width, q, per)
        x = arrived[:, q * MAIN : (q + 1) * MAIN, :].reshape(sources * MAIN, part)
        pick = (col == row // EXTRA * few + q * EXTRA + row % EXTRA).astype(F32).astype(BF)
        y = dot(pick, tail).astype(BF)
        if q == 0:
            acc_main[...] = dot_nt(x, both)
            acc_extra[...] = dot_nt(y, both)
        else:
            acc_main[...] += dot_nt(x, both)
            acc_extra[...] += dot_nt(y, both)
    for acc, hid in ((acc_main, hid_main), (acc_extra, hid_extra)):
        gate = acc[:, :width]
        hid[...] = (gate / (1.0 + jnp.exp(-gate)) * acc[:, width:]).astype(BF)
    row = iota((sources * few, sources * EXTRA), 0)
    col = iota((sources * few, sources * EXTRA), 1)
    back = jnp.zeros((sources * few, part), F32)
    for q in range(QUARTERS):
        down = lanes(w, 2 * width, 3 * width, q, per)
        out = dot(hid_main[...], down).astype(BF)
        answered[:, q * MAIN : (q + 1) * MAIN, :] = out.reshape(sources, MAIN, part)
        few_out = dot(hid_extra[...], down).astype(BF)
        put = (row == col // EXTRA * few + q * EXTRA + col % EXTRA).astype(F32).astype(BF)
        back = back + dot(put, few_out)
    answered[:, QUARTERS * MAIN :, :] = back.reshape(sources, few, part).astype(BF)


def shared_body(normed, w, out):
    devices, three, features = w.shape
    few = three // 3
    parts = [w[:, i * few : (i + 1) * few, :].reshape(devices * few, features) for i in range(3)]
    n = normed[...]
    gate = dot_nt(n, parts[0])
    up = dot_nt(n, parts[1])
    hidden = (gate / (1.0 + jnp.exp(-gate)) * up).astype(BF)
    out[...] = dot(hidden, parts[2])


def split_weight(w):
    high = w.astype(BF)
    return high, (w - high.astype(F32)).astype(BF)


def combine_body(returned, routes, route_weight, shared, mixed):
    experts = returned.shape[0]
    part = returned.shape[2]
    few = QUARTERS * EXTRA
    rows, top = routes.shape
    raw = route_weight[...]
    weights = raw / jnp.sum(raw, axis=1, keepdims=True) * ROUTED_SCALE
    ids = [routes[:, k : k + 1] for k in range(top)]
    hot = [(iota((rows, experts), 1) == ids[k]).astype(F32) for k in range(top)]
    named = sum(hot[1:], hot[0])
    earlier = (iota((rows, rows), 1) < iota((rows, rows), 0)).astype(BF)
    before = dot(earlier, named.astype(BF))
    ranks = [jnp.sum(before * h, axis=1, keepdims=True).astype(jnp.int32) for h in hot]
    spot = iota((rows, experts * MAIN), 1)
    main = jnp.zeros((rows, experts * MAIN), F32)
    for k in range(top):
        target = jnp.where(ranks[k] < MAIN, ids[k] * MAIN + ranks[k], -1)
        main = jnp.where(spot == target, weights[:, k : k + 1], main)
    high, low = split_weight(main)
    spot = iota((rows, experts * few), 1)
    tail = returned[:, QUARTERS * MAIN :, :].astype(F32).reshape(experts * few, part).astype(BF)
    for q in range(QUARTERS):
        x = returned[:, q * MAIN : (q + 1) * MAIN, :].reshape(experts * MAIN, part)
        pick = jnp.zeros((rows, experts * few), F32)
        for k in range(top):
            slot = ids[k] * few + q * EXTRA + ranks[k] - MAIN
            slot = jnp.where(ranks[k] < MAIN, -1, slot)
            pick = jnp.where(spot == slot, weights[:, k : k + 1], pick)
        pick_high, pick_low = split_weight(pick)
        routed = dot(high, x) + dot(low, x) + dot(pick_high, tail) + dot(pick_low, tail)
        at = slice(q * part, (q + 1) * part)
        mixed[:, at] = (shared[:, at] + routed).astype(BF)


def local(tokens, gain, ex_gate, ex_up, ex_down, sh_gate, sh_up, sh_down, routes, route_weight):
    rows, features = tokens.shape
    top = routes.shape[1]
    hidden, block = ex_gate.shape[1:]
    few = sh_gate.shape[0]
    parts = lax.axis_size("fs")
    experts = lax.axis_size(TP)
    part = features // QUARTERS
    shape = jax.ShapeDtypeStruct

    with jax.named_scope("fold"):
        args = (gain[None, :], ex_gate, ex_up, ex_down, sh_gate, sh_up, sh_down)
        out = (shape((3 * hidden, block), BF), shape((3 * hidden + 3 * few, block), BF))
        routed_w, both_w = call(fold_body, out, args, 10**6, "fold")
    with jax.named_scope("zgather"):
        over_z = lax.all_gather(routed_w, "tp_0", axis=0, tiled=False)
    with jax.named_scope("own"):
        copies = jnp.broadcast_to(both_w[None], (parts,) + both_w.shape)
        own = lax.all_to_all(copies, "fs", 0, 0, tiled=True)
    with jax.named_scope("place"):
        size = MAIN * QUARTERS + EXTRA * QUARTERS
        out = (shape((experts, size, part), BF), shape((rows, features), BF))
        flops = 2 * rows * features * experts * (MAIN + EXTRA)
        outgoing, normed = call(place_body, out, (tokens, routes.T), flops, "place")
    with jax.named_scope("send"):
        arrived = lax.all_to_all(outgoing, PLANE, 0, 0, tiled=True)
    with jax.named_scope("ownout"):
        own = jnp.moveaxis(own, 0, 1).reshape(-1, features)
        exp_gate, exp_up, exp_down = (own[i * hidden : (i + 1) * hidden][None] for i in range(3))
        shr = own[3 * hidden :]
        shr_gate, shr_up, shr_down = (shr[i * few : (i + 1) * few] for i in range(3))
    with jax.named_scope("shgather"):
        shared_w = lax.all_gather(shr, TP, axis=0, tiled=False)
    with jax.named_scope("weights"):
        expert_w = lax.all_to_all(over_z, "fs", 0, 0, tiled=True)
    with jax.named_scope("experts"):
        n = experts * MAIN
        m = experts * EXTRA
        out = shape(outgoing.shape, BF)
        answered = pl.pallas_call(
            expert_body,
            out_shape=out,
            in_specs=[whole(arrived.shape), whole(expert_w.shape)],
            out_specs=whole(out.shape),
            scratch_shapes=[
                pltpu.VMEM((n, 2 * hidden), F32),
                pltpu.VMEM((m, 2 * hidden), F32),
                pltpu.VMEM((n, hidden), BF),
                pltpu.VMEM((m, hidden), BF),
            ],
            cost_estimate=pl.CostEstimate(
                flops=6 * (n + m) * hidden * features, bytes_accessed=8 * 10**6, transcendentals=0
            ),
            name="experts",
        )(arrived, expert_w)
    with jax.named_scope("back"):
        returned = lax.all_to_all(answered, PLANE, 0, 0, tiled=True)
    with jax.named_scope("shared"):
        out = (shape((rows, features), F32),)
        (shared,) = call(shared_body, out, (normed, shared_w), 6 * rows * features * few * experts, "shared")
    with jax.named_scope("combine"):
        out = (shape((rows, features), BF),)
        args = (returned, routes, route_weight, shared)
        (mixed,) = call(combine_body, out, args, 4 * rows * features * (n + m), "combine")
    return (mixed, exp_gate, exp_up, exp_down, shr_gate, shr_up, shr_down)


def solution(mesh):
    split = Mesh(mesh.devices.reshape(mesh.shape["fs"], 16, 2), ("fs", "tp_0", "tp_1"))
    in_specs = (
        P(FS_TP, None),
        P("fs"),
        P(TP, None, "fs"),
        P(TP, None, "fs"),
        P(TP, None, "fs"),
        P(TP, "fs"),
        P(TP, "fs"),
        P(TP, "fs"),
        P(FS_TP, None),
        P(FS_TP, None),
    )
    out_specs = (
        P(FS_TP, None),
        P(TP, None, None),
        P(TP, None, None),
        P(TP, None, None),
        P(TP, None),
        P(TP, None),
        P(TP, None),
    )
    return jax.shard_map(local, mesh=split, in_specs=in_specs, out_specs=out_specs, check_vma=False)
```

time: 367 us -> 209 us (0.57)
  the two profiles are of different devices: /device:TPU:46 before, /device:TPU:320 now
where the time goes in v1:
time: 209 us
  blocking collectives  130 us (62%)
  local copies, waits for them, and re-layouts  29.4 us (14%)
  Pallas kernels  23.3 us (11%)
  between operations  14.1 us (7%)
  waiting for transfers between devices  7.8 us (4%)
  starting transfers between devices  4.27 us (2%)
    all_to_all x1, blocking collectives, local(): own = lax.all_to_all(copies, 'fs', 0, 0, tiled=True)  48.6 us
    all_to_all x1, blocking collectives, local(): expert_w = lax.all_to_all(over_z, 'fs', 0, 0, tiled=True)  45.2 us
    all_to_all x1, blocking collectives, local(): arrived = lax.all_to_all(outgoing, PLANE, 0, 0, tiled=True)  36 us
    pallas_call x4, Pallas kernels, call(): pl.pallas_call(body, out_shape=out, in_specs=[whole(a.shape) for a in arg...  15.8 us
    unnamed x11, local copies, waits for them, and re-layouts  8.84 us
    slice x4, local copies, waits for them, and re-layouts, local(): shr_gate, shr_up, shr_down = (shr[i * few:(i + 1) * few] for i in range(3))  8.6 us
    all_to_all x1, waiting for transfers between devices, local(): returned = lax.all_to_all(answered, PLANE, 0, 0, tiled=True)  7.77 us
    pallas_call x1, Pallas kernels, local(): pl.pallas_call(expert_body, out_shape=out, in_specs=[whole(arrived.shape)...  7.51 us
  transfers between devices with their start and end apart: 3, of which 1 were waited for; matrix products, arithmetic and copies ran while one was open for 13% of the time, Pallas kernels for 8%

profile of v1, /device:TPU:320, one launch (start us, length us, event | category | flops | bytes accessed | tf_op | source)
XLA Modules:
  0.0 208.6 jit_solution(7213194616991178623)
XLA Ops:
  7.2 0.0 all-gather.6.cloned.1.call-start
  7.2 1.8 fold.1
  9.1 0.0 all-gather.6.cloned.1.call-update
  9.1 0.0 all-gather.4.cloned.1.call-start
  9.1 1.4 broadcast_in_dim.19
  10.5 48.6 %all_to_all.20 = bf16[16,816,128]{2,1,0:T(8,128)(2,1)S(1)} all-to-all(bf16[16,816,128]{2,1,0:T(8,128)(2,1)S(1)} %broadcast_in_dim.19), channel_id=1, replica_groups=mesh['fs'=16,'tp_0'=16,'tp_1'=2] {'fs'}, dimensions={0} | all-to-all | bytes 6684672 | tf_op jit(solution)/shard_map/own/all_to_all | solution.py:213
  59.1 5.1 %copy.21 = bf16[16,816,128]{1,2,0:T(8,128)(2,1)} copy(bf16[16,816,128]{2,1,0:T(8,128)(2,1)S(1)} %all_to_all.20) | data formatting | bytes 6684672 | tf_op jit(solution)/shard_map/own/all_to_all | solution.py:213
  64.2 1.1 slice.47
  65.2 0.9 copy.31
  66.1 0.0 all-gather.4.cloned.1.call-update
  66.1 3.6 %place.1 = (bf16[32,72,512]{2,1,0:T(8,128)(2,1)}, bf16[128,2048]{1,0:T(8,128)(2,1)}) custom-call(bf16[128,2048]{1,0:T(8,128)(2,1)} %tokens.1, s32[4,128]{1,0:T(4,128)} %bitcast.22), custom_call_target="tpu_custom_call" | custom-call | flops 301989888 | bytes 3409920 | tf_op jit(solution)/shard_map/place/place/pallas_call | solution.py:44
  69.8 36.0 %all_to_all.21.arrived = bf16[32,72,512]{2,1,0:T(8,128)(2,1)} all-to-all(bf16[32,72,512]{2,1,0:T(8,128)(2,1)} %get-tuple-element.11), channel_id=1, replica_groups=mesh['fs'=16,'tp_0'=16,'tp_1'=2] {'fs','tp_1'}, dimensions={0} | all-to-all | bytes 4718592 | tf_op jit(solution)/shard_map/send/all_to_all | solution.py:220
  105.8 0.0 all-gather.6.cloned.1.call-done
  105.8 45.2 %all_to_all.22.w = bf16[16,768,128]{2,1,0:T(8,128)(2,1)} all-to-all(bf16[16,768,128]{2,1,0:T(8,128)(2,1)} %bitcast.17), channel_id=1, replica_groups=mesh['fs'=16,'tp_0'=16,'tp_1'=2] {'fs'}, dimensions={0} | all-to-all | bytes 6291456 | tf_op jit(solution)/shard_map/weights/all_to_all | solution.py:229
  151.0 7.5 %experts.1 = bf16[32,72,512]{2,1,0:T(8,128)(2,1)} custom-call(bf16[32,72,512]{2,1,0:T(8,128)(2,1)} %all_to_all.21.arrived, bf16[16,768,128]{2,1,0:T(8,128)(2,1)} %all_to_all.22.w), custom_call_target="tpu_custom_call" | custom-call | flops 1811939328 | bytes 8000000 | tf_op jit(solution)/shard_map/experts/experts/pallas_call | solution.py:234
  158.5 0.0 copy-start.1
  158.5 0.0 copy-start.2
  158.5 4.2 %all-to-all-start.2 = ((bf16[32,72,512]{2,1,0:T(8,128)(2,1)}), bf16[32,72,512]{2,1,0:T(8,128)(2,1)S(1)}, u32[]{:S(2)}, u32[]{:S(2)}) async-start(bf16[32,72,512]{2,1,0:T(8,128)(2,1)} %experts.1), calls=%async_computation.2 | async-start | bytes 4718592 | tf_op jit(solution)/shard_map/back/all_to_all | solution.py:251
  162.7 0.0 copy-done.1
  162.7 0.7 copy.23.routes
  163.4 0.0 copy-done.2
  163.4 0.7 copy.24.route_weight
  164.2 3.5 %fusion.1 = (bf16[256,16,128]{0,2,1:T(8,128)(2,1)}, bf16[256,16,128]{0,2,1:T(8,128)(2,1)}, bf16[256,16,128]{0,2,1:T(8,128)(2,1)S(1)}) fusion(bf16[816,16,128]{0,2,1:T(8,128)(2,1)} %bitcast.12), kind=kLoop, calls=%fused_computation.1 | loop fusion | bytes 6291456 | tf_op jit(solution)/shard_map/ownout/slice | solution.py:223
  167.7 2.3 %copy.30 = bf16[1,256,2048]{2,1,0:T(8,128)(2,1)} copy(bf16[1,256,2048]{1,2,0:T(8,128)(2,1)} %bitcast.16) | data formatting | bytes 2097152
  169.9 2.3 %copy.29 = bf16[1,256,2048]{2,1,0:T(8,128)(2,1)} copy(bf16[1,256,2048]{1,2,0:T(8,128)(2,1)} %bitcast.15) | data formatting | bytes 2097152
  172.2 3.1 %fusion = (bf16[16,16,128]{0,2,1:T(8,128)(2,1)}, bf16[16,16,128]{0,2,1:T(8,128)(2,1)}, bf16[16,16,128]{0,2,1:T(8,128)(2,1)}) fusion(bf16[816,16,128]{0,2,1:T(8,128)(2,1)} %bitcast.13), kind=kLoop, calls=%fused_computation | loop fusion | bytes 393216 | tf_op jit(solution)/shard_map/ownout/slice | solution.py:225
  175.2 1.8 copy.34
  177.1 1.8 copy.33
  178.9 1.8 copy.32
  180.8 1.4 copy.28
  182.2 0.0 all-gather.4.cloned.1.call-done.w
  182.2 5.9 %shared.1 = f32[128,2048]{1,0:T(8,128)} custom-call(bf16[128,2048]{1,0:T(8,128)(2,1)} %get-tuple-element.13.normed, bf16[32,48,2048]{2,1,0:T(8,128)(2,1)} %all-gather.4.cloned.1.call-done.w), custom_call_target="tpu_custom_call" | custom-call | flops 805306368 | bytes 7864320 | tf_op jit(solution)/shard_map/shared/shared/pallas_call | solution.py:44
  188.1 7.8 %all-to-all-done.2.returned = bf16[32,72,512]{2,1,0:T(8,128)(2,1)S(1)} async-done(((bf16[32,72,512]{2,1,0:T(8,128)(2,1)}), bf16[32,72,512]{2,1,0:T(8,128)(2,1)S(1)}, u32[]{:S(2)}, u32[]{:S(2)}) %all-to-all-start.2) | async-done | bytes 2359328 | tf_op jit(solution)/shard_map/back/all_to_all | solution.py:251
  195.8 0.0 copy-start
  195.8 1.4 copy-done
  197.3 4.5 %combine.1 = bf16[128,2048]{1,0:T(8,128)(2,1)} custom-call(bf16[32,72,512]{2,1,0:T(8,128)(2,1)} %copy-done, s32[128,4]{1,0:T(8,128)} %copy.23.routes, f32[128,4]{1,0:T(8,128)} %copy.24.route_weight, f32[128,2048]{1,0:T(8,128)} %shared.1), custom_call_target="tpu_custom_call" | custom-call | flops 603979776 | bytes 3936256 | tf_op jit(solution)/shard_map/combine/combine/pallas_call | solution.py:44
Async XLA Ops:
  7.2 98.6 %all-gather.6.cloned.1.call-start = ((), (), s32[]{:S(2)}) async-start(), calls=%async_computation.5 | async-start | bytes 3342336 | tf_op jit(solution)/shard_map/zgather/all_gather | solution.py:210
  9.1 173.1 %all-gather.4.cloned.1.call-start = ((), (), s32[]{:S(2)}) async-start(), calls=%async_computation.4 | async-start | bytes 6488064 | tf_op jit(solution)/shard_map/shgather/all_gather | solution.py:227
  158.5 4.2 %copy-start.1 = (s32[128,4]{0,1:T(4,128)S(1)}, s32[128,4]{0,1:T(4,128)}, u32[]{:S(2)}) copy-start(s32[128,4]{0,1:T(4,128)} %param.18) | copy-start | bytes 6148
  158.5 4.9 %copy-start.2 = (f32[128,4]{0,1:T(4,128)S(1)}, f32[128,4]{0,1:T(4,128)}, u32[]{:S(2)}) copy-start(f32[128,4]{0,1:T(4,128)} %param.19) | copy-start | bytes 6148
  158.5 37.4 %all-to-all-start.2 = ((bf16[32,72,512]{2,1,0:T(8,128)(2,1)}), bf16[32,72,512]{2,1,0:T(8,128)(2,1)S(1)}, u32[]{:S(2)}, u32[]{:S(2)}) async-start(bf16[32,72,512]{2,1,0:T(8,128)(2,1)} %experts.1), calls=%async_computation.2 | async-start | bytes 4718592 | tf_op jit(solution)/shard_map/back/all_to_all | solution.py:251
  195.8 1.4 copy-start
Sparse Core Ops, SparseCore 0:
  10.6 71.8 all-gather.5
  84.6 72.7 all-gather.3

commit v2 on v1

v2 whole, which is shorter than its diff:
```python
import jax
import jax.numpy as jnp
from jax import lax
from jax.experimental import pallas as pl
from jax.experimental.pallas import tpu as pltpu
from jax.sharding import Mesh
from jax.sharding import PartitionSpec as P


TP = ("tp_0", "tp_1")
FS = ("y", "x")
PLANE = FS + ("tp_1",)
FS_TP = FS + TP


EPS = 1e-06
ROUTED_SCALE = 2.5
BF = jnp.bfloat16
F32 = jnp.float32
NT = (((1,), (1,)), ((), ()))

MAIN = 16
EXTRA = 2
QUARTERS = 4
GRANT = 24 << 20


def dot(a, b):
    return jnp.dot(a, b, preferred_element_type=F32)


def dot_nt(a, b):
    return lax.dot_general(a, b, NT, preferred_element_type=F32)


def iota(shape, dim):
    return lax.broadcasted_iota(jnp.int32, shape, dim)


def whole(shape):
    return pl.BlockSpec(shape, lambda *_: (0,) * len(shape))


def call(body, out, args, flops, limit=None, specs=None, grid=(), scratch=()):
    moved = sum(a.size * a.dtype.itemsize for a in args) + sum(o.size * o.dtype.itemsize for o in out)
    return pl.pallas_call(
        body,
        grid=grid,
        out_shape=out,
        in_specs=specs or [whole(a.shape) for a in args],
        out_specs=[whole(o.shape) for o in out],
        scratch_shapes=list(scratch),
        cost_estimate=pl.CostEstimate(flops=flops, bytes_accessed=moved, transcendentals=0),
        compiler_params=pltpu.CompilerParams(vmem_limit_bytes=limit),
    )(*args)


def fold_body(gain, eg, eu, ed, sg, su, sd, routed, first, second):
    scale = gain[...]
    at = 0
    cut = second.shape[0]
    for part in (eg[0] * scale, eu[0] * scale, ed[0]):
        middle = part.shape[0] // 2
        for piece in (part[:middle].astype(BF), part[middle:].astype(BF)):
            rows = piece.shape[0]
            routed[at : at + rows, :] = piece
            if at < cut:
                first[at : at + rows, :] = piece
            else:
                second[at - cut : at - cut + rows, :] = piece
            at += rows
    at = cut
    for part in (sg[...] * scale, su[...] * scale, sd[...]):
        first[at : at + part.shape[0], :] = part.astype(BF)
        at += part.shape[0]


def place_body(tokens, routes_t, outgoing, normed_out):
    values = tokens[...].astype(F32)
    mean = jnp.mean(values * values, axis=1, keepdims=True)
    normed = (values * lax.rsqrt(mean + EPS)).astype(BF)
    normed_out[...] = normed
    experts = outgoing.shape[0]
    top, rows = routes_t.shape
    ids = [routes_t[k : k + 1, :] for k in range(top)]
    hot = [(iota((experts, rows), 0) == ids[k]).astype(F32) for k in range(top)]
    named = sum(hot[1:], hot[0])
    earlier = (iota((rows, rows), 0) < iota((rows, rows), 1)).astype(BF)
    before = dot(named.astype(BF), earlier)
    ranks = [jnp.sum(before * h, axis=0, keepdims=True).astype(jnp.int32) for h in hot]
    spot = iota((experts * MAIN, rows), 0)
    main = jnp.zeros((experts * MAIN, rows), F32)
    for k in range(top):
        target = jnp.where(ranks[k] < MAIN, ids[k] * MAIN + ranks[k], -1)
        main = jnp.where(spot == target, 1.0, main)
    main = main.astype(BF)
    few = QUARTERS * EXTRA
    spot = iota((experts * few, rows), 0)
    part = normed.shape[1] // QUARTERS
    extra = jnp.zeros((experts * few, part), F32)
    for q in range(QUARTERS):
        piece = normed[:, q * part : (q + 1) * part]
        rows_q = dot(main, piece).astype(BF)
        outgoing[:, q * MAIN : (q + 1) * MAIN, :] = rows_q.reshape(experts, MAIN, part)
        pick = jnp.zeros((experts * few, rows), F32)
        for k in range(top):
            slot = ids[k] * few + q * EXTRA + ranks[k] - MAIN
            pick = jnp.where(spot == jnp.where(ranks[k] < MAIN, -1, slot), 1.0, pick)
        extra = extra + dot(pick.astype(BF), piece)
    outgoing[:, QUARTERS * MAIN :, :] = extra.reshape(experts, few, part).astype(BF)


def lanes(w, lo, hi, q, per):
    return jnp.concatenate([w[q * per + i, lo:hi, :] for i in range(per)], axis=1)


def expert_body(arrived, w, answered, acc_main, acc_extra, hid_main, hid_extra):
    sources = arrived.shape[0]
    part = arrived.shape[2]
    per = part // w.shape[2]
    width = w.shape[1] // 3
    few = QUARTERS * EXTRA
    tail = arrived[:, QUARTERS * MAIN :, :].astype(F32).reshape(sources * few, part).astype(BF)
    row = iota((sources * EXTRA, sources * few), 0)
    col = iota((sources * EXTRA, sources * few), 1)
    for q in range(QUARTERS):
        both = lanes(w, 0, 2 * width, q, per)
        x = arrived[:, q * MAIN : (q + 1) * MAIN, :].reshape(sources * MAIN, part)
        pick = (col == row // EXTRA * few + q * EXTRA + row % EXTRA).astype(F32).astype(BF)
        y = dot(pick, tail).astype(BF)
        if q == 0:
            acc_main[...] = dot_nt(x, both)
            acc_extra[...] = dot_nt(y, both)
        else:
            acc_main[...] += dot_nt(x, both)
            acc_extra[...] += dot_nt(y, both)
    for acc, hid in ((acc_main, hid_main), (acc_extra, hid_extra)):
        gate = acc[:, :width]
        hid[...] = (gate / (1.0 + jnp.exp(-gate)) * acc[:, width:]).astype(BF)
    row = iota((sources * few, sources * EXTRA), 0)
    col = iota((sources * few, sources * EXTRA), 1)
    back = jnp.zeros((sources * few, part), F32)
    for q in range(QUARTERS):
        down = lanes(w, 2 * width, 3 * width, q, per)
        out = dot(hid_main[...], down).astype(BF)
        answered[:, q * MAIN : (q + 1) * MAIN, :] = out.reshape(sources, MAIN, part)
        few_out = dot(hid_extra[...], down).astype(BF)
        put = (row == col // EXTRA * few + q * EXTRA + col % EXTRA).astype(F32).astype(BF)
        back = back + dot(put, few_out)
    answered[:, QUARTERS * MAIN :, :] = back.reshape(sources, few, part).astype(BF)


def shared_body(normed, w, out):
    devices, three, features = w.shape
    few = three // 3
    parts = [w[:, i * few : (i + 1) * few, :].reshape(devices * few, features) for i in range(3)]
    n = normed[...]
    gate = dot_nt(n, parts[0])
    up = dot_nt(n, parts[1])
    hidden = (gate / (1.0 + jnp.exp(-gate)) * up).astype(BF)
    out[...] = dot(hidden, parts[2])


def split_weight(w):
    high = w.astype(BF)
    return high, (w - high.astype(F32)).astype(BF)


def mixers_body(routes, route_weight, main_high, main_low, few_high, few_low):
    rows, top = routes.shape
    few = QUARTERS * EXTRA
    experts = main_high.shape[1] // MAIN
    raw = route_weight[...]
    weights = raw / jnp.sum(raw, axis=1, keepdims=True) * ROUTED_SCALE
    ids = [routes[:, k : k + 1] for k in range(top)]
    hot = [(iota((rows, experts), 1) == ids[k]).astype(F32) for k in range(top)]
    named = sum(hot[1:], hot[0])
    earlier = (iota((rows, rows), 1) < iota((rows, rows), 0)).astype(BF)
    before = dot(earlier, named.astype(BF))
    ranks = [jnp.sum(before * h, axis=1, keepdims=True).astype(jnp.int32) for h in hot]
    spot = iota((rows, experts * MAIN), 1)
    main = jnp.zeros((rows, experts * MAIN), F32)
    for k in range(top):
        target = jnp.where(ranks[k] < MAIN, ids[k] * MAIN + ranks[k], -1)
        main = jnp.where(spot == target, weights[:, k : k + 1], main)
    main_high[...], main_low[...] = split_weight(main)
    spot = iota((rows, experts * few), 1)
    for q in range(QUARTERS):
        pick = jnp.zeros((rows, experts * few), F32)
        for k in range(top):
            slot = ids[k] * few + q * EXTRA + ranks[k] - MAIN
            slot = jnp.where(ranks[k] < MAIN, -1, slot)
            pick = jnp.where(spot == slot, weights[:, k : k + 1], pick)
        few_high[q], few_low[q] = split_weight(pick)


def combine_body(returned, main_high, main_low, few_high, few_low, shared_hbm, mixed, shared, sem):
    fetch = pltpu.make_async_copy(shared_hbm, shared, sem)
    fetch.start()
    experts = returned.shape[0]
    part = returned.shape[2]
    few = QUARTERS * EXTRA
    tail = returned[:, QUARTERS * MAIN :, :].astype(F32).reshape(experts * few, part).astype(BF)
    for q in range(QUARTERS):
        x = returned[:, q * MAIN : (q + 1) * MAIN, :].reshape(experts * MAIN, part)
        routed = dot(main_high[...], x) + dot(main_low[...], x)
        routed = routed + dot(few_high[q], tail) + dot(few_low[q], tail)
        if q == 0:
            fetch.wait()
        at = slice(q * part, (q + 1) * part)
        mixed[:, at] = (shared[:, at] + routed).astype(BF)


def swapped(array, axis, other):
    pairs = [(i, i ^ other) for i in range(lax.axis_size(axis))]
    return lax.ppermute(array, axis, pairs) if other else array


def place_of(index, other, block):
    return pl.ds(pl.multiple_of((index[0] ^ other) * block, block), block)


def few_body(index, *refs):
    stacks, out = refs[:-1], refs[-1]
    side, rows, block = stacks[0].shape
    for j, stack in enumerate(stacks):
        for k in range(side):
            out[:, place_of(index, j * side + k, block)] = stack[k, rows - out.shape[0] :, :]


def split_body(index, shr, *refs):
    outs = refs[-6:]
    side = (len(refs) - 6) // 2
    first, second = refs[:side], refs[side : 2 * side]
    gate, up, down = outs[:3]
    rows = gate.shape[1]
    half = rows // 2
    block = first[0].shape[2]
    for i in range(side):
        for j in range(side):
            at = place_of(index, i * side + j, block)
            gate[0, :, at] = first[i][j, :rows, :]
            up[0, :half, at] = first[i][j, rows : rows + half, :]
            up[0, half:, at] = second[j][i, :half, :]
            down[0, :, at] = second[j][i, half : half + rows, :]
    for i, ref in enumerate(outs[3:]):
        ref[...] = shr[i * ref.shape[0] : (i + 1) * ref.shape[0], :]


def step(tokens, gain, ex_gate, ex_up, ex_down, sh_gate, sh_up, sh_down, routes, route_weight):
    rows, features = tokens.shape
    hidden, block = ex_gate.shape[1:]
    few = sh_gate.shape[0]
    experts = lax.axis_size(TP)
    part = features // QUARTERS
    shape = jax.ShapeDtypeStruct

    args = (gain[None, :], ex_gate, ex_up, ex_down, sh_gate, sh_up, sh_down)
    cut = 3 * hidden // 2
    out = (shape((2 * cut, block), BF), shape((cut + 3 * few, block), BF), shape((cut, block), BF))
    routed_w, first_w, second_w = call(fold_body, out, args, 10**6)
    over_z = lax.all_gather(routed_w, "tp_0", axis=0, tiled=False)
    size = MAIN * QUARTERS + EXTRA * QUARTERS
    out = (shape((experts, size, part), BF), shape((rows, features), BF))
    flops = 2 * rows * features * experts * (MAIN + EXTRA)
    outgoing, normed = call(place_body, out, (tokens, routes.T), flops)
    arrived = lax.all_to_all(outgoing, PLANE, 0, 0, tiled=True)
    side = lax.axis_size("x")
    first = [swapped(first_w, "x", k) for k in range(side)]
    second = [swapped(second_w, "y", k) for k in range(side)]
    first, second = jnp.stack(first), jnp.stack(second)
    firsts = [swapped(first, "y", k) for k in range(side)]
    index = lax.axis_index(FS).astype(jnp.int32).reshape(1)
    scalar = [pl.BlockSpec(memory_space=pltpu.SMEM)]
    out = (shape((3 * few, features), BF),)
    specs = scalar + [whole(first.shape)] * side
    (shr,) = call(few_body, out, (index, *firsts), 10**6, None, specs)
    shared_w = lax.all_gather(shr, TP, axis=0, tiled=False)
    seconds = [swapped(second, "x", k) for k in range(side)]
    out = (shape((1, hidden, features), BF),) * 3 + (shape((few, features), BF),) * 3
    specs = scalar + [whole(shr.shape)] + [whole(first.shape)] * side + [whole(second.shape)] * side
    outs = call(split_body, out, (index, shr, *firsts, *seconds), 10**7, None, specs)
    expert_w = lax.all_to_all(over_z, FS, 0, 0, tiled=True)
    n = experts * MAIN
    m = experts * EXTRA
    out = shape(outgoing.shape, BF)
    answered = pl.pallas_call(
        expert_body,
        out_shape=out,
        in_specs=[whole(arrived.shape), whole(expert_w.shape)],
        out_specs=whole(out.shape),
        scratch_shapes=[
            pltpu.VMEM((n, 2 * hidden), F32),
            pltpu.VMEM((m, 2 * hidden), F32),
            pltpu.VMEM((n, hidden), BF),
            pltpu.VMEM((m, hidden), BF),
        ],
        cost_estimate=pl.CostEstimate(
            flops=6 * (n + m) * hidden * features, bytes_accessed=8 * 10**6, transcendentals=0
        ),
        compiler_params=pltpu.CompilerParams(vmem_limit_bytes=GRANT),
        name="experts",
    )(arrived, expert_w)
    returned = lax.all_to_all(answered, PLANE, 0, 0, tiled=True)
    out = (shape((rows, n), BF),) * 2 + (shape((QUARTERS, rows, m * QUARTERS), BF),) * 2
    mixers = call(mixers_body, out, (routes, route_weight), 10**7)
    out = (shape((rows, features), F32),)
    (shared,) = call(shared_body, out, (normed, shared_w), 6 * rows * features * few * experts)
    out = (shape((rows, features), BF),)
    args = (returned, *mixers, shared)
    specs = [whole(a.shape) for a in args[:-1]] + [pl.BlockSpec(memory_space=pltpu.HBM)]
    scratch = [pltpu.VMEM((rows, features), F32), pltpu.SemaphoreType.DMA(())]
    (mixed,) = call(
        combine_body, out, args, 4 * rows * features * (n + m), GRANT, specs, (), scratch
    )
    return (mixed, *outs)


def solution(mesh):
    split = Mesh(mesh.devices.reshape(4, 4, 16, 2), FS_TP)
    in_specs = (
        P(FS_TP, None),
        P(FS),
        P(TP, None, FS),
        P(TP, None, FS),
        P(TP, None, FS),
        P(TP, FS),
        P(TP, FS),
        P(TP, FS),
        P(FS_TP, None),
        P(FS_TP, None),
    )
    out_specs = (
        P(FS_TP, None),
        P(TP, None, None),
        P(TP, None, None),
        P(TP, None, None),
        P(TP, None),
        P(TP, None),
        P(TP, None),
    )
    return jax.shard_map(step, mesh=split, in_specs=in_specs, out_specs=out_specs, check_vma=False)
```

time: 209 us -> 235 us (1.12)
  the two profiles are of different devices: /device:TPU:320 before, /device:TPU:288 now
where the time goes in v2:
time: 235 us
  blocking collectives  79.7 us (34%)
  waiting for transfers between devices  63.7 us (27%)
  starting transfers between devices  44.8 us (19%)
  Pallas kernels  26.2 us (11%)
  between operations  14.3 us (6%)
  local copies, waits for them, and re-layouts  4.95 us (2%)
    ppermute x12, waiting for transfers between devices, swapped(): return lax.ppermute(array, axis, pairs) if other else array  63.7 us
    all_to_all x1, blocking collectives, step(): expert_w = lax.all_to_all(over_z, FS, 0, 0, tiled=True)  44.3 us
    ppermute x12, starting transfers between devices, swapped(): return lax.ppermute(array, axis, pairs) if other else array  40.5 us
    all_to_all x1, blocking collectives, step(): arrived = lax.all_to_all(outgoing, PLANE, 0, 0, tiled=True)  35.4 us
    pallas_call x7, Pallas kernels, call(): pl.pallas_call(body, grid=grid, out_shape=out, in_specs=specs or [whole(a...  22.7 us
    unnamed x34, local copies, waits for them, and re-layouts  4.95 us
  transfers between devices with their start and end apart: 15, of which 8 were waited for; matrix products, arithmetic and copies ran while one was open for 1% of the time, Pallas kernels for 10%

profile of v2, /device:TPU:288, one launch (start us, length us, event | category | flops | bytes accessed | tf_op | source)
XLA Modules:
  0.0 234.6 jit_solution(5277380757634614935)
XLA Ops:
  7.2 0.0 all-gather.5.cloned.1.call-start
  7.2 1.8 shard_map.154
  9.0 0.0 all-gather.5.cloned.1.call-update
  9.1 0.0 all-gather.7.cloned.1.call-start
  9.1 4.7 %collective-permute-start.2 = (bf16[432,128]{1,0:T(8,128)(2,1)}, bf16[432,128]{1,0:T(8,128)(2,1)S(1)}, u32[]{:S(2)}, u32[]{:S(2)}) collective-permute-start(bf16[432,128]{1,0:T(8,128)(2,1)} %get-tuple-element.29), channel_id=1, source_target_pairs={{0,96},{32,64},{64,32},{96,0},{1,97},{33,65},{65,33},{97,1},{2,98}... | collective-permute-start | bytes 331784 | tf_op jit(solution)/shard_map/ppermute | solution.py:216
  13.8 2.7 %collective-permute-start.1 = (bf16[432,128]{1,0:T(8,128)(2,1)}, bf16[432,128]{1,0:T(8,128)(2,1)S(1)}, u32[]{:S(2)}, u32[]{:S(2)}) collective-permute-start(bf16[432,128]{1,0:T(8,128)(2,1)} %get-tuple-element.29), channel_id=1, source_target_pairs={{0,64},{32,96},{64,0},{96,32},{1,65},{33,97},{65,1},{97,33},{2,66}... | collective-permute-start | bytes 331784 | tf_op jit(solution)/shard_map/ppermute | solution.py:216
  16.5 2.4 %collective-permute-start = (bf16[432,128]{1,0:T(8,128)(2,1)}, bf16[432,128]{1,0:T(8,128)(2,1)S(1)}, u32[]{:S(2)}, u32[]{:S(2)}) collective-permute-start(bf16[432,128]{1,0:T(8,128)(2,1)} %get-tuple-element.29), channel_id=1, source_target_pairs={{0,32},{32,0},{64,96},{96,64},{1,33},{33,1},{65,97},{97,65},{2,34}... | collective-permute-start | bytes 331784 | tf_op jit(solution)/shard_map/ppermute | solution.py:216
  19.0 0.0 collective-permute-done.2
  19.0 3.3 %collective-permute-done.1 = bf16[432,128]{1,0:T(8,128)(2,1)S(1)} collective-permute-done((bf16[432,128]{1,0:T(8,128)(2,1)}, bf16[432,128]{1,0:T(8,128)(2,1)S(1)}, u32[]{:S(2)}, u32[]{:S(2)}) %collective-permute-start.1) | collective-permute-done | bytes 110624 | tf_op jit(solution)/shard_map/ppermute | solution.py:216
  22.3 1.1 collective-permute-done
  23.4 1.0 pad_maximum_fusion.refs_0_
  24.3 3.5 %collective-permute-start.3 = (bf16[4,432,128]{2,1,0:T(8,128)(2,1)S(1)}, bf16[4,432,128]{2,1,0:T(8,128)(2,1)S(1)}, u32[]{:S(2)}, u32[]{:S(2)}) collective-permute-start(bf16[4,432,128]{2,1,0:T(8,128)(2,1)S(1)} %pad_maximum_fusion.refs_0_), channel_id=1, source_target_pairs={{0,128},{128,0},{256,384},{384,256},{1,129},{129,1},{257,385},{385... | collective-permute-start | bytes 1327112 | tf_op jit(solution)/shard_map/ppermute | solution.py:216
  27.8 4.8 %collective-permute-start.4 = (bf16[4,432,128]{2,1,0:T(8,128)(2,1)S(1)}, bf16[4,432,128]{2,1,0:T(8,128)(2,1)S(1)}, u32[]{:S(2)}, u32[]{:S(2)}) collective-permute-start(bf16[4,432,128]{2,1,0:T(8,128)(2,1)S(1)} %pad_maximum_fusion.refs_0_), channel_id=1, source_target_pairs={{0,256},{128,384},{256,0},{384,128},{1,257},{129,385},{257,1},{385... | collective-permute-start | bytes 1327112 | tf_op jit(solution)/shard_map/ppermute | solution.py:216
  32.6 2.1 collective-permute-start.5
  34.8 4.5 %collective-permute-done.3.refs_1_ = bf16[4,432,128]{2,1,0:T(8,128)(2,1)S(1)} collective-permute-done((bf16[4,432,128]{2,1,0:T(8,128)(2,1)S(1)}, bf16[4,432,128]{2,1,0:T(8,128)(2,1)S(1)}, u32[]{:S(2)}, u32[]{:S(2)}) %collective-permute-start.3) | collective-permute-done | bytes 442400 | tf_op jit(solution)/shard_map/ppermute | solution.py:216
  39.3 9.5 %collective-permute-done.4.refs_2_ = bf16[4,432,128]{2,1,0:T(8,128)(2,1)S(1)} collective-permute-done((bf16[4,432,128]{2,1,0:T(8,128)(2,1)S(1)}, bf16[4,432,128]{2,1,0:T(8,128)(2,1)S(1)}, u32[]{:S(2)}, u32[]{:S(2)}) %collective-permute-start.4) | collective-permute-done | bytes 442400 | tf_op jit(solution)/shard_map/ppermute | solution.py:216
  48.7 6.4 %collective-permute-done.5.refs_3_ = bf16[4,432,128]{2,1,0:T(8,128)(2,1)S(1)} collective-permute-done((bf16[4,432,128]{2,1,0:T(8,128)(2,1)S(1)}, bf16[4,432,128]{2,1,0:T(8,128)(2,1)S(1)}, u32[]{:S(2)}, u32[]{:S(2)}) %collective-permute-start.5) | collective-permute-done | bytes 442400 | tf_op jit(solution)/shard_map/ppermute | solution.py:216
  55.2 0.7 copy-done.9
  55.9 2.1 shard_map.156.shr
  58.0 0.0 all-gather.7.cloned.1.call-update
  58.1 3.6 %shard_map.153 = (bf16[32,72,512]{2,1,0:T(8,128)(2,1)}, bf16[128,2048]{1,0:T(8,128)(2,1)}) custom-call(bf16[128,2048]{1,0:T(8,128)(2,1)} %tokens.1, s32[4,128]{1,0:T(4,128)} %bitcast.23), custom_call_target="tpu_custom_call" | custom-call | flops 301989888 | bytes 3409920 | tf_op jit(solution)/shard_map/pallas_call | solution.py:46
  61.7 35.4 %all_to_all.15.arrived = bf16[32,72,512]{2,1,0:T(8,128)(2,1)S(1)} all-to-all(bf16[32,72,512]{2,1,0:T(8,128)(2,1)} %get-tuple-element.22), channel_id=1, replica_groups=mesh['y'=4,'x'=4,'tp_0'=16,'tp_1'=2] {'y','x','tp_1'}, dimensions={0} | all-to-all | bytes 4718592 | tf_op jit(solution)/shard_map/all_to_all | solution.py:267
  97.1 44.3 %all_to_all.16.w = bf16[16,768,128]{2,1,0:T(8,128)(2,1)S(1)} all-to-all(bf16[16,768,128]{2,1,0:T(8,128)(2,1)} %bitcast.14), channel_id=1, replica_groups=mesh['y'=4,'x'=4,'tp_0'=16,'tp_1'=2] {'y','x'}, dimensions={0} | all-to-all | bytes 6291456 | tf_op jit(solution)/shard_map/all_to_all | solution.py:283
  141.4 3.4 %experts.1 = bf16[32,72,512]{2,1,0:T(8,128)(2,1)S(1)} custom-call(bf16[32,72,512]{2,1,0:T(8,128)(2,1)S(1)} %all_to_all.15.arrived, bf16[16,768,128]{2,1,0:T(8,128)(2,1)S(1)} %all_to_all.16.w), custom_call_target="tpu_custom_call" | custom-call | flops 1811939328 | bytes 8000000 | tf_op jit(solution)/shard_map/experts/pallas_call | solution.py:287
  144.8 1.5 copy-done
  146.3 4.2 %all-to-all-start.2 = ((bf16[32,72,512]{2,1,0:T(8,128)(2,1)}), bf16[32,72,512]{2,1,0:T(8,128)(2,1)S(1)}, u32[]{:S(2)}, u32[]{:S(2)}) async-start(bf16[32,72,512]{2,1,0:T(8,128)(2,1)} %copy-done), calls=%async_computation.2 | async-start | bytes 4718592 | tf_op jit(solution)/shard_map/all_to_all | solution.py:304
  150.5 5.0 %collective-permute-start.8 = (bf16[384,128]{1,0:T(8,128)(2,1)S(1)}, bf16[384,128]{1,0:T(8,128)(2,1)S(1)}, u32[]{:S(2)}, u32[]{:S(2)}) collective-permute-start(bf16[384,128]{1,0:T(8,128)(2,1)S(1)} %copy-done.13), channel_id=1, source_target_pairs={{0,384},{128,256},{256,128},{384,0},{1,385},{129,257},{257,129},{3... | collective-permute-start | bytes 294920 | tf_op jit(solution)/shard_map/ppermute | solution.py:216
  155.5 2.7 %collective-permute-start.7 = (bf16[384,128]{1,0:T(8,128)(2,1)S(1)}, bf16[384,128]{1,0:T(8,128)(2,1)S(1)}, u32[]{:S(2)}, u32[]{:S(2)}) collective-permute-start(bf16[384,128]{1,0:T(8,128)(2,1)S(1)} %copy-done.13), channel_id=1, source_target_pairs={{0,256},{128,384},{256,0},{384,128},{1,257},{129,385},{257,1},{385... | collective-permute-start | bytes 294920 | tf_op jit(solution)/shard_map/ppermute | solution.py:216
  158.1 2.2 collective-permute-start.6
  160.4 23.8 %collective-permute-done.8 = bf16[384,128]{1,0:T(8,128)(2,1)S(1)} collective-permute-done((bf16[384,128]{1,0:T(8,128)(2,1)S(1)}, bf16[384,128]{1,0:T(8,128)(2,1)S(1)}, u32[]{:S(2)}, u32[]{:S(2)}) %collective-permute-start.8) | collective-permute-done | bytes 98336 | tf_op jit(solution)/shard_map/ppermute | solution.py:216
  184.1 0.0 collective-permute-done.7
  184.1 0.0 collective-permute-done.6
  184.1 0.1 pad_maximum_fusion.1.refs_4_
  184.2 0.0 copy-start.10
  184.2 3.4 %collective-permute-start.9 = (bf16[4,384,128]{2,1,0:T(8,128)(2,1)S(1)}, bf16[4,384,128]{2,1,0:T(8,128)(2,1)S(1)}, u32[]{:S(2)}, u32[]{:S(2)}) collective-permute-start(bf16[4,384,128]{2,1,0:T(8,128)(2,1)S(1)} %pad_maximum_fusion.1.refs_4_), channel_id=1, source_target_pairs={{0,32},{32,0},{64,96},{96,64},{1,33},{33,1},{65,97},{97,65},{2,34}... | collective-permute-start | bytes 1179656 | tf_op jit(solution)/shard_map/ppermute | solution.py:216
  187.6 4.6 %collective-permute-start.10 = (bf16[4,384,128]{2,1,0:T(8,128)(2,1)S(1)}, bf16[4,384,128]{2,1,0:T(8,128)(2,1)S(1)}, u32[]{:S(2)}, u32[]{:S(2)}) collective-permute-start(bf16[4,384,128]{2,1,0:T(8,128)(2,1)S(1)} %pad_maximum_fusion.1.refs_4_), channel_id=1, source_target_pairs={{0,64},{32,96},{64,0},{96,32},{1,65},{33,97},{65,1},{97,33},{2,66}... | collective-permute-start | bytes 1179656 | tf_op jit(solution)/shard_map/ppermute | solution.py:216
  192.2 2.4 %collective-permute-start.11 = (bf16[4,384,128]{2,1,0:T(8,128)(2,1)S(1)}, bf16[4,384,128]{2,1,0:T(8,128)(2,1)}, u32[]{:S(2)}, u32[]{:S(2)}) collective-permute-start(bf16[4,384,128]{2,1,0:T(8,128)(2,1)S(1)} %pad_maximum_fusion.1.refs_4_), channel_id=1, source_target_pairs={{0,96},{32,64},{64,32},{96,0},{1,97},{33,65},{65,33},{97,1},{2,98}... | collective-permute-start | bytes 1179656 | tf_op jit(solution)/shard_map/ppermute | solution.py:216
  194.6 0.7 copy.17.routes
  195.4 0.7 copy.18.route_weight
  196.1 2.7 %shard_map.155 = (bf16[128,512]{1,0:T(8,128)(2,1)}, bf16[128,512]{1,0:T(8,128)(2,1)}, bf16[4,128,256]{2,1,0:T(8,128)(2,1)}, bf16[4,128,256]{2,1,0:T(8,128)(2,1)}) custom-call(s32[128,4]{1,0:T(8,128)} %copy.17.routes, f32[128,4]{1,0:T(8,128)} %copy.18.route_weight), custom_call_target="tpu_custom_call" | custom-call | flops 10000000 | bytes 790528 | tf_op jit(solution)/shard_map/pallas_call | solution.py:46
  198.9 0.0 collective-permute-done.9.refs_5_
  198.9 8.6 %collective-permute-done.10.refs_6_ = bf16[4,384,128]{2,1,0:T(8,128)(2,1)S(1)} collective-permute-done((bf16[4,384,128]{2,1,0:T(8,128)(2,1)S(1)}, bf16[4,384,128]{2,1,0:T(8,128)(2,1)S(1)}, u32[]{:S(2)}, u32[]{:S(2)}) %collective-permute-start.10) | collective-permute-done | bytes 393248 | tf_op jit(solution)/shard_map/ppermute | solution.py:216
  207.5 6.5 %collective-permute-done.11.refs_7_ = bf16[4,384,128]{2,1,0:T(8,128)(2,1)} collective-permute-done((bf16[4,384,128]{2,1,0:T(8,128)(2,1)S(1)}, bf16[4,384,128]{2,1,0:T(8,128)(2,1)}, u32[]{:S(2)}, u32[]{:S(2)}) %collective-permute-start.11) | collective-permute-done | bytes 393248 | tf_op jit(solution)/shard_map/ppermute | solution.py:216
  214.0 4.5 %shard_map.159 = (bf16[1,256,2048]{2,1,0:T(8,128)(2,1)}, bf16[1,256,2048]{2,1,0:T(8,128)(2,1)}, bf16[1,256,2048]{2,1,0:T(8,128)(2,1)}, bf16[16,2048]{1,0:T(8,128...) custom-call(s32[1]{0:T(128)} %bitcast.3.index, bf16[48,2048]{1,0:T(8,128)(2,1)} %shard_map.156.shr, ...), custom_call_target="tpu_custom_call" | custom-call | flops 10000000 | bytes 6881284 | tf_op jit(solution)/shard_map/pallas_call | solution.py:46
  218.6 5.9 %shard_map.157.shared_hbm = f32[128,2048]{1,0:T(8,128)} custom-call(bf16[128,2048]{1,0:T(8,128)(2,1)} %get-tuple-element.28.normed, bf16[32,48,2048]{2,1,0:T(8,128)(2,1)} %bitcast.13), custom_call_target="tpu_custom_call" | custom-call | flops 805306368 | bytes 7864320 | tf_op jit(solution)/shard_map/pallas_call | solution.py:46
  224.5 0.0 all-to-all-done.2.returned
  224.5 1.2 copy-done.1
  225.7 2.0 shard_map.158
  (30 shorter events, 0.1 us)
Async XLA Ops:
  7.2 89.9 %all-gather.5.cloned.1.call-start = ((), (), s32[]{:S(2)}) async-start(), calls=%async_computation.3 | async-start | bytes 3342336 | tf_op jit(solution)/shard_map/all_gather | solution.py:262
  9.1 209.5 %all-gather.7.cloned.1.call-start = ((), (), s32[]{:S(2)}) async-start(), calls=%async_computation.4 | async-start | bytes 6488064 | tf_op jit(solution)/shard_map/all_gather | solution.py:278
  9.1 9.8 %collective-permute-start.2 = (bf16[432,128]{1,0:T(8,128)(2,1)}, bf16[432,128]{1,0:T(8,128)(2,1)S(1)}, u32[]{:S(2)}, u32[]{:S(2)}) collective-permute-start(bf16[432,128]{1,0:T(8,128)(2,1)} %get-tuple-element.29), channel_id=1, source_target_pairs={{0,96},{32,64},{64,32},{96,0},{1,97},{33,65},{65,33},{97,1},{2,98}... | collective-permute-start | bytes 331784 | tf_op jit(solution)/shard_map/ppermute | solution.py:216
  13.8 8.5 %collective-permute-start.1 = (bf16[432,128]{1,0:T(8,128)(2,1)}, bf16[432,128]{1,0:T(8,128)(2,1)S(1)}, u32[]{:S(2)}, u32[]{:S(2)}) collective-permute-start(bf16[432,128]{1,0:T(8,128)(2,1)} %get-tuple-element.29), channel_id=1, source_target_pairs={{0,64},{32,96},{64,0},{96,32},{1,65},{33,97},{65,1},{97,33},{2,66}... | collective-permute-start | bytes 331784 | tf_op jit(solution)/shard_map/ppermute | solution.py:216
  16.5 6.9 %collective-permute-start = (bf16[432,128]{1,0:T(8,128)(2,1)}, bf16[432,128]{1,0:T(8,128)(2,1)S(1)}, u32[]{:S(2)}, u32[]{:S(2)}) collective-permute-start(bf16[432,128]{1,0:T(8,128)(2,1)} %get-tuple-element.29), channel_id=1, source_target_pairs={{0,32},{32,0},{64,96},{96,64},{1,33},{33,1},{65,97},{97,65},{2,34}... | collective-permute-start | bytes 331784 | tf_op jit(solution)/shard_map/ppermute | solution.py:216
  24.3 30.8 %copy-start.6 = (bf16[4,432,128]{2,1,0:T(8,128)(2,1)}, bf16[4,432,128]{2,1,0:T(8,128)(2,1)S(1)}, u32[]{:S(2)}) copy-start(bf16[4,432,128]{2,1,0:T(8,128)(2,1)S(1)} %pad_maximum_fusion.refs_0_) | copy-start | bytes 1327108
  24.3 14.9 %collective-permute-start.3 = (bf16[4,432,128]{2,1,0:T(8,128)(2,1)S(1)}, bf16[4,432,128]{2,1,0:T(8,128)(2,1)S(1)}, u32[]{:S(2)}, u32[]{:S(2)}) collective-permute-start(bf16[4,432,128]{2,1,0:T(8,128)(2,1)S(1)} %pad_maximum_fusion.refs_0_), channel_id=1, source_target_pairs={{0,128},{128,0},{256,384},{384,256},{1,129},{129,1},{257,385},{385... | collective-permute-start | bytes 1327112 | tf_op jit(solution)/shard_map/ppermute | solution.py:216
  27.8 20.9 %collective-permute-start.4 = (bf16[4,432,128]{2,1,0:T(8,128)(2,1)S(1)}, bf16[4,432,128]{2,1,0:T(8,128)(2,1)S(1)}, u32[]{:S(2)}, u32[]{:S(2)}) collective-permute-start(bf16[4,432,128]{2,1,0:T(8,128)(2,1)S(1)} %pad_maximum_fusion.refs_0_), channel_id=1, source_target_pairs={{0,256},{128,384},{256,0},{384,128},{1,257},{129,385},{257,1},{385... | collective-permute-start | bytes 1327112 | tf_op jit(solution)/shard_map/ppermute | solution.py:216
  32.6 22.5 %collective-permute-start.5 = (bf16[4,432,128]{2,1,0:T(8,128)(2,1)S(1)}, bf16[4,432,128]{2,1,0:T(8,128)(2,1)S(1)}, u32[]{:S(2)}, u32[]{:S(2)}) collective-permute-start(bf16[4,432,128]{2,1,0:T(8,128)(2,1)S(1)} %pad_maximum_fusion.refs_0_), channel_id=1, source_target_pairs={{0,384},{128,256},{256,128},{384,0},{1,385},{129,257},{257,129},{3... | collective-permute-start | bytes 1327112 | tf_op jit(solution)/shard_map/ppermute | solution.py:216
  39.3 15.9 %copy-start.7 = (bf16[4,432,128]{2,1,0:T(8,128)(2,1)}, bf16[4,432,128]{2,1,0:T(8,128)(2,1)S(1)}, u32[]{:S(2)}) copy-start(bf16[4,432,128]{2,1,0:T(8,128)(2,1)S(1)} %collective-permute-done.3.refs_1_) | copy-start | bytes 1327108
  48.7 6.4 %copy-start.8 = (bf16[4,432,128]{2,1,0:T(8,128)(2,1)}, bf16[4,432,128]{2,1,0:T(8,128)(2,1)S(1)}, u32[]{:S(2)}) copy-start(bf16[4,432,128]{2,1,0:T(8,128)(2,1)S(1)} %collective-permute-done.4.refs_2_) | copy-start | bytes 1327108
  55.2 0.8 copy-start.9
  144.8 1.5 copy-start
  146.3 4.2 %copy-start.13 = (bf16[384,128]{1,0:T(8,128)(2,1)S(1)}, bf16[384,128]{1,0:T(8,128)(2,1)}, u32[]{:S(2)}) copy-start(bf16[384,128]{1,0:T(8,128)(2,1)} %get-tuple-element.30) | copy-start | bytes 294916
  146.3 48.3 %copy-start.14 = (s32[128,4]{0,1:T(4,128)S(1)}, s32[128,4]{0,1:T(4,128)}, u32[]{:S(2)}) copy-start(s32[128,4]{0,1:T(4,128)} %param.18) | copy-start | bytes 6148
  146.3 49.1 %copy-start.15 = (f32[128,4]{0,1:T(4,128)S(1)}, f32[128,4]{0,1:T(4,128)}, u32[]{:S(2)}) copy-start(f32[128,4]{0,1:T(4,128)} %param.19) | copy-start | bytes 6148
  146.3 78.2 %all-to-all-start.2 = ((bf16[32,72,512]{2,1,0:T(8,128)(2,1)}), bf16[32,72,512]{2,1,0:T(8,128)(2,1)S(1)}, u32[]{:S(2)}, u32[]{:S(2)}) async-start(bf16[32,72,512]{2,1,0:T(8,128)(2,1)} %copy-done), calls=%async_computation.2 | async-start | bytes 4718592 | tf_op jit(solution)/shard_map/all_to_all | solution.py:304
  150.5 33.6 %collective-permute-start.8 = (bf16[384,128]{1,0:T(8,128)(2,1)S(1)}, bf16[384,128]{1,0:T(8,128)(2,1)S(1)}, u32[]{:S(2)}, u32[]{:S(2)}) collective-permute-start(bf16[384,128]{1,0:T(8,128)(2,1)S(1)} %copy-done.13), channel_id=1, source_target_pairs={{0,384},{128,256},{256,128},{384,0},{1,385},{129,257},{257,129},{3... | collective-permute-start | bytes 294920 | tf_op jit(solution)/shard_map/ppermute | solution.py:216
  155.5 28.6 %collective-permute-start.7 = (bf16[384,128]{1,0:T(8,128)(2,1)S(1)}, bf16[384,128]{1,0:T(8,128)(2,1)S(1)}, u32[]{:S(2)}, u32[]{:S(2)}) collective-permute-start(bf16[384,128]{1,0:T(8,128)(2,1)S(1)} %copy-done.13), channel_id=1, source_target_pairs={{0,256},{128,384},{256,0},{384,128},{1,257},{129,385},{257,1},{385... | collective-permute-start | bytes 294920 | tf_op jit(solution)/shard_map/ppermute | solution.py:216
  158.1 26.0 %collective-permute-start.6 = (bf16[384,128]{1,0:T(8,128)(2,1)S(1)}, bf16[384,128]{1,0:T(8,128)(2,1)S(1)}, u32[]{:S(2)}, u32[]{:S(2)}) collective-permute-start(bf16[384,128]{1,0:T(8,128)(2,1)S(1)} %copy-done.13), channel_id=1, source_target_pairs={{0,128},{128,0},{256,384},{384,256},{1,129},{129,1},{257,385},{385... | collective-permute-start | bytes 294920 | tf_op jit(solution)/shard_map/ppermute | solution.py:216
  184.2 29.9 %copy-start.10 = (bf16[4,384,128]{2,1,0:T(8,128)(2,1)}, bf16[4,384,128]{2,1,0:T(8,128)(2,1)S(1)}, u32[]{:S(2)}) copy-start(bf16[4,384,128]{2,1,0:T(8,128)(2,1)S(1)} %pad_maximum_fusion.1.refs_4_) | copy-start | bytes 1179652
  184.2 14.7 %collective-permute-start.9 = (bf16[4,384,128]{2,1,0:T(8,128)(2,1)S(1)}, bf16[4,384,128]{2,1,0:T(8,128)(2,1)S(1)}, u32[]{:S(2)}, u32[]{:S(2)}) collective-permute-start(bf16[4,384,128]{2,1,0:T(8,128)(2,1)S(1)} %pad_maximum_fusion.1.refs_4_), channel_id=1, source_target_pairs={{0,32},{32,0},{64,96},{96,64},{1,33},{33,1},{65,97},{97,65},{2,34}... | collective-permute-start | bytes 1179656 | tf_op jit(solution)/shard_map/ppermute | solution.py:216
  187.6 19.9 %collective-permute-start.10 = (bf16[4,384,128]{2,1,0:T(8,128)(2,1)S(1)}, bf16[4,384,128]{2,1,0:T(8,128)(2,1)S(1)}, u32[]{:S(2)}, u32[]{:S(2)}) collective-permute-start(bf16[4,384,128]{2,1,0:T(8,128)(2,1)S(1)} %pad_maximum_fusion.1.refs_4_), channel_id=1, source_target_pairs={{0,64},{32,96},{64,0},{96,32},{1,65},{33,97},{65,1},{97,33},{2,66}... | collective-permute-start | bytes 1179656 | tf_op jit(solution)/shard_map/ppermute | solution.py:216
  192.2 21.8 %collective-permute-start.11 = (bf16[4,384,128]{2,1,0:T(8,128)(2,1)S(1)}, bf16[4,384,128]{2,1,0:T(8,128)(2,1)}, u32[]{:S(2)}, u32[]{:S(2)}) collective-permute-start(bf16[4,384,128]{2,1,0:T(8,128)(2,1)S(1)} %pad_maximum_fusion.1.refs_4_), channel_id=1, source_target_pairs={{0,96},{32,64},{64,32},{96,0},{1,97},{33,65},{65,33},{97,1},{2,98}... | collective-permute-start | bytes 1179656 | tf_op jit(solution)/shard_map/ppermute | solution.py:216
  198.9 15.2 %copy-start.11 = (bf16[4,384,128]{2,1,0:T(8,128)(2,1)}, bf16[4,384,128]{2,1,0:T(8,128)(2,1)S(1)}, u32[]{:S(2)}) copy-start(bf16[4,384,128]{2,1,0:T(8,128)(2,1)S(1)} %collective-permute-done.9.refs_5_) | copy-start | bytes 1179652
  207.5 6.5 %copy-start.12 = (bf16[4,384,128]{2,1,0:T(8,128)(2,1)}, bf16[4,384,128]{2,1,0:T(8,128)(2,1)S(1)}, u32[]{:S(2)}) copy-start(bf16[4,384,128]{2,1,0:T(8,128)(2,1)S(1)} %collective-permute-done.10.refs_6_) | copy-start | bytes 1179652
  218.6 5.9 %copy-start.2 = (bf16[4,128,256]{2,1,0:T(8,128)(2,1)S(1)}, bf16[4,128,256]{2,1,0:T(8,128)(2,1)}, u32[]{:S(2)}) copy-start(bf16[4,128,256]{2,1,0:T(8,128)(2,1)} %get-tuple-element.26.few_high) | copy-start | bytes 786436
  218.6 5.9 %copy-start.3 = (bf16[4,128,256]{2,1,0:T(8,128)(2,1)S(1)}, bf16[4,128,256]{2,1,0:T(8,128)(2,1)}, u32[]{:S(2)}) copy-start(bf16[4,128,256]{2,1,0:T(8,128)(2,1)} %get-tuple-element.27.few_low) | copy-start | bytes 786436
  218.6 5.9 %copy-start.4 = (bf16[128,512]{1,0:T(8,128)(2,1)S(1)}, bf16[128,512]{1,0:T(8,128)(2,1)}, u32[]{:S(2)}) copy-start(bf16[128,512]{1,0:T(8,128)(2,1)} %get-tuple-element.24.main_high) | copy-start | bytes 393220
  218.6 5.9 %copy-start.5 = (bf16[128,512]{1,0:T(8,128)(2,1)S(1)}, bf16[128,512]{1,0:T(8,128)(2,1)}, u32[]{:S(2)}) copy-start(bf16[128,512]{1,0:T(8,128)(2,1)} %get-tuple-element.25.main_low) | copy-start | bytes 393220
  224.5 1.2 copy-start.1
Sparse Core Ops, SparseCore 0:
  10.6 71.8 all-gather.4
  84.6 73.1 all-gather.6

commit v3 on v2

--- a/solution.py
+++ b/solution.py
@@ -266,9 +266,10 @@
     outgoing, normed = call(place_body, out, (tokens, routes.T), flops)
     arrived = lax.all_to_all(outgoing, PLANE, 0, 0, tiled=True)
     side = lax.axis_size("x")
-    first = [swapped(first_w, "x", k) for k in range(side)]
-    second = [swapped(second_w, "y", k) for k in range(side)]
-    first, second = jnp.stack(first), jnp.stack(second)
+    first = jnp.stack([first_w, swapped(first_w, "x", 1)])
+    second = jnp.stack([second_w, swapped(second_w, "y", 1)])
+    first = jnp.concatenate([first, swapped(first, "x", 2)])
+    second = jnp.concatenate([second, swapped(second, "y", 2)])
     firsts = [swapped(first, "y", k) for k in range(side)]
     index = lax.axis_index(FS).astype(jnp.int32).reshape(1)
     scalar = [pl.BlockSpec(memory_space=pltpu.SMEM)]

time: 235 us -> 244 us (1.038)
  the two profiles are of different devices: /device:TPU:288 before, /device:TPU:224 now
where the time goes in v3:
time: 244 us; the launch traced here: 243 us
  blocking collectives  80.4 us (33%)
  waiting for transfers between devices  74 us (30%)
  starting transfers between devices  41.5 us (17%)
  Pallas kernels  26.2 us (11%)
  between operations  14.3 us (6%)
  local copies, waits for them, and re-layouts  4.95 us (2%)
    ppermute x10, waiting for transfers between devices, swapped(): return lax.ppermute(array, axis, pairs) if other else array  74 us
    all_to_all x1, blocking collectives, step(): expert_w = lax.all_to_all(over_z, FS, 0, 0, tiled=True)  44.4 us
    ppermute x10, starting transfers between devices, swapped(): return lax.ppermute(array, axis, pairs) if other else array  37.2 us
    all_to_all x1, blocking collectives, step(): arrived = lax.all_to_all(outgoing, PLANE, 0, 0, tiled=True)  36 us
    pallas_call x7, Pallas kernels, call(): pl.pallas_call(body, grid=grid, out_shape=out, in_specs=specs or [whole(a...  22.8 us
    unnamed x34, local copies, waits for them, and re-layouts  4.95 us
  transfers between devices with their start and end apart: 13, of which 9 were waited for; matrix products, arithmetic and copies ran while one was open for 1% of the time, Pallas kernels for 9%

profile of v3, /device:TPU:224, one launch (start us, length us, event | category | flops | bytes accessed | tf_op | source)
XLA Modules:
  0.0 243.2 jit_solution(12545688960104914193)
XLA Ops:
  7.2 0.0 all-gather.5.cloned.1.call-start
  7.2 1.8 shard_map.154
  9.0 0.0 all-gather.5.cloned.1.call-update
  9.1 0.0 all-gather.7.cloned.1.call-start
  9.1 3.4 %collective-permute-start = (bf16[432,128]{1,0:T(8,128)(2,1)}, bf16[432,128]{1,0:T(8,128)(2,1)S(1)}, u32[]{:S(2)}, u32[]{:S(2)}) collective-permute-start(bf16[432,128]{1,0:T(8,128)(2,1)} %get-tuple-element.29), channel_id=1, source_target_pairs={{0,32},{32,0},{64,96},{96,64},{1,33},{33,1},{65,97},{97,65},{2,34}... | collective-permute-start | bytes 331784 | tf_op jit(solution)/shard_map/ppermute | solution.py:216
  12.5 3.5 %collective-permute-done = bf16[432,128]{1,0:T(8,128)(2,1)S(1)} collective-permute-done((bf16[432,128]{1,0:T(8,128)(2,1)}, bf16[432,128]{1,0:T(8,128)(2,1)S(1)}, u32[]{:S(2)}, u32[]{:S(2)}) %collective-permute-start) | collective-permute-done | bytes 110624 | tf_op jit(solution)/shard_map/ppermute | solution.py:216
  16.0 0.9 pad_maximum_fusion.2
  16.9 4.9 %collective-permute-start.1 = (bf16[2,432,128]{2,1,0:T(8,128)(2,1)S(1)}, bf16[2,432,128]{2,1,0:T(8,128)(2,1)S(1)}, u32[]{:S(2)}, u32[]{:S(2)}) collective-permute-start(bf16[2,432,128]{2,1,0:T(8,128)(2,1)S(1)} %pad_maximum_fusion.2), channel_id=1, source_target_pairs={{0,64},{32,96},{64,0},{96,32},{1,65},{33,97},{65,1},{97,33},{2,66}... | collective-permute-start | bytes 663560 | tf_op jit(solution)/shard_map/ppermute | solution.py:216
  21.9 4.8 %collective-permute-done.1 = bf16[2,432,128]{2,1,0:T(8,128)(2,1)S(1)} collective-permute-done((bf16[2,432,128]{2,1,0:T(8,128)(2,1)S(1)}, bf16[2,432,128]{2,1,0:T(8,128)(2,1)S(1)}, u32[]{:S(2)}, u32[]{:S(2)}) %collective-permute-start.1) | collective-permute-done | bytes 221216 | tf_op jit(solution)/shard_map/ppermute | solution.py:216
  26.7 0.9 pad_maximum_fusion.refs_0_
  27.6 0.0 copy-start.6
  27.6 3.5 %collective-permute-start.2 = (bf16[4,432,128]{2,1,0:T(8,128)(2,1)S(1)}, bf16[4,432,128]{2,1,0:T(8,128)(2,1)S(1)}, u32[]{:S(2)}, u32[]{:S(2)}) collective-permute-start(bf16[4,432,128]{2,1,0:T(8,128)(2,1)S(1)} %pad_maximum_fusion.refs_0_), channel_id=1, source_target_pairs={{0,128},{128,0},{256,384},{384,256},{1,129},{129,1},{257,385},{385... | collective-permute-start | bytes 1327112 | tf_op jit(solution)/shard_map/ppermute | solution.py:216
  31.1 4.8 %collective-permute-start.3 = (bf16[4,432,128]{2,1,0:T(8,128)(2,1)S(1)}, bf16[4,432,128]{2,1,0:T(8,128)(2,1)S(1)}, u32[]{:S(2)}, u32[]{:S(2)}) collective-permute-start(bf16[4,432,128]{2,1,0:T(8,128)(2,1)S(1)} %pad_maximum_fusion.refs_0_), channel_id=1, source_target_pairs={{0,256},{128,384},{256,0},{384,128},{1,257},{129,385},{257,1},{385... | collective-permute-start | bytes 1327112 | tf_op jit(solution)/shard_map/ppermute | solution.py:216
  35.9 2.1 collective-permute-start.4
  38.1 4.5 %collective-permute-done.2.refs_1_ = bf16[4,432,128]{2,1,0:T(8,128)(2,1)S(1)} collective-permute-done((bf16[4,432,128]{2,1,0:T(8,128)(2,1)S(1)}, bf16[4,432,128]{2,1,0:T(8,128)(2,1)S(1)}, u32[]{:S(2)}, u32[]{:S(2)}) %collective-permute-start.2) | collective-permute-done | bytes 442400 | tf_op jit(solution)/shard_map/ppermute | solution.py:216
  42.5 9.2 %collective-permute-done.3.refs_2_ = bf16[4,432,128]{2,1,0:T(8,128)(2,1)S(1)} collective-permute-done((bf16[4,432,128]{2,1,0:T(8,128)(2,1)S(1)}, bf16[4,432,128]{2,1,0:T(8,128)(2,1)S(1)}, u32[]{:S(2)}, u32[]{:S(2)}) %collective-permute-start.3) | collective-permute-done | bytes 442400 | tf_op jit(solution)/shard_map/ppermute | solution.py:216
  51.7 6.4 %collective-permute-done.4.refs_3_ = bf16[4,432,128]{2,1,0:T(8,128)(2,1)S(1)} collective-permute-done((bf16[4,432,128]{2,1,0:T(8,128)(2,1)S(1)}, bf16[4,432,128]{2,1,0:T(8,128)(2,1)S(1)}, u32[]{:S(2)}, u32[]{:S(2)}) %collective-permute-start.4) | collective-permute-done | bytes 442400 | tf_op jit(solution)/shard_map/ppermute | solution.py:216
  58.1 0.0 copy-done.6
  58.1 0.0 copy-done.7
  58.2 0.7 copy-done.9
  58.9 2.1 shard_map.156.shr
  61.0 0.0 all-gather.7.cloned.1.call-update
  61.0 3.6 %shard_map.153 = (bf16[32,72,512]{2,1,0:T(8,128)(2,1)}, bf16[128,2048]{1,0:T(8,128)(2,1)}) custom-call(bf16[128,2048]{1,0:T(8,128)(2,1)} %tokens.1, s32[4,128]{1,0:T(4,128)} %bitcast.19), custom_call_target="tpu_custom_call" | custom-call | flops 301989888 | bytes 3409920 | tf_op jit(solution)/shard_map/pallas_call | solution.py:46
  64.7 36.0 %all_to_all.15.arrived = bf16[32,72,512]{2,1,0:T(8,128)(2,1)S(1)} all-to-all(bf16[32,72,512]{2,1,0:T(8,128)(2,1)} %get-tuple-element.22), channel_id=1, replica_groups=mesh['y'=4,'x'=4,'tp_0'=16,'tp_1'=2] {'y','x','tp_1'}, dimensions={0} | all-to-all | bytes 4718592 | tf_op jit(solution)/shard_map/all_to_all | solution.py:267
  100.6 44.4 %all_to_all.16.w = bf16[16,768,128]{2,1,0:T(8,128)(2,1)S(1)} all-to-all(bf16[16,768,128]{2,1,0:T(8,128)(2,1)} %bitcast.10), channel_id=1, replica_groups=mesh['y'=4,'x'=4,'tp_0'=16,'tp_1'=2] {'y','x'}, dimensions={0} | all-to-all | bytes 6291456 | tf_op jit(solution)/shard_map/all_to_all | solution.py:284
  145.0 3.4 %experts.1 = bf16[32,72,512]{2,1,0:T(8,128)(2,1)S(1)} custom-call(bf16[32,72,512]{2,1,0:T(8,128)(2,1)S(1)} %all_to_all.15.arrived, bf16[16,768,128]{2,1,0:T(8,128)(2,1)S(1)} %all_to_all.16.w), custom_call_target="tpu_custom_call" | custom-call | flops 1811939328 | bytes 8000000 | tf_op jit(solution)/shard_map/experts/pallas_call | solution.py:288
  148.5 0.0 copy-start
  148.5 1.5 copy-done
  150.0 4.2 %all-to-all-start.2 = ((bf16[32,72,512]{2,1,0:T(8,128)(2,1)}), bf16[32,72,512]{2,1,0:T(8,128)(2,1)S(1)}, u32[]{:S(2)}, u32[]{:S(2)}) async-start(bf16[32,72,512]{2,1,0:T(8,128)(2,1)} %copy-done), calls=%async_computation.2 | async-start | bytes 4718592 | tf_op jit(solution)/shard_map/all_to_all | solution.py:305
  154.2 3.6 %collective-permute-start.5 = (bf16[384,128]{1,0:T(8,128)(2,1)S(1)}, bf16[384,128]{1,0:T(8,128)(2,1)S(1)}, u32[]{:S(2)}, u32[]{:S(2)}) collective-permute-start(bf16[384,128]{1,0:T(8,128)(2,1)S(1)} %copy-done.11), channel_id=1, source_target_pairs={{0,128},{128,0},{256,384},{384,256},{1,129},{129,1},{257,385},{385... | collective-permute-start | bytes 294920 | tf_op jit(solution)/shard_map/ppermute | solution.py:216
  157.8 26.2 %collective-permute-done.5 = bf16[384,128]{1,0:T(8,128)(2,1)S(1)} collective-permute-done((bf16[384,128]{1,0:T(8,128)(2,1)S(1)}, bf16[384,128]{1,0:T(8,128)(2,1)S(1)}, u32[]{:S(2)}, u32[]{:S(2)}) %collective-permute-start.5) | collective-permute-done | bytes 98336 | tf_op jit(solution)/shard_map/ppermute | solution.py:216
  184.0 4.4 %collective-permute-start.6 = (bf16[2,384,128]{2,1,0:T(8,128)(2,1)S(1)}, bf16[2,384,128]{2,1,0:T(8,128)(2,1)S(1)}, u32[]{:S(2)}, u32[]{:S(2)}) collective-permute-start(bf16[2,384,128]{2,1,0:T(8,128)(2,1)S(1)} %pad_maximum_fusion.3), channel_id=1, source_target_pairs={{0,256},{128,384},{256,0},{384,128},{1,257},{129,385},{257,1},{385... | collective-permute-start | bytes 589832 | tf_op jit(solution)/shard_map/ppermute | solution.py:216
  188.4 5.3 %collective-permute-done.6 = bf16[2,384,128]{2,1,0:T(8,128)(2,1)S(1)} collective-permute-done((bf16[2,384,128]{2,1,0:T(8,128)(2,1)S(1)}, bf16[2,384,128]{2,1,0:T(8,128)(2,1)S(1)}, u32[]{:S(2)}, u32[]{:S(2)}) %collective-permute-start.6) | collective-permute-done | bytes 196640 | tf_op jit(solution)/shard_map/ppermute | solution.py:216
  193.8 2.4 %collective-permute-start.7 = (bf16[4,384,128]{2,1,0:T(8,128)(2,1)S(1)}, bf16[4,384,128]{2,1,0:T(8,128)(2,1)S(1)}, u32[]{:S(2)}, u32[]{:S(2)}) collective-permute-start(bf16[4,384,128]{2,1,0:T(8,128)(2,1)S(1)} %pad_maximum_fusion.1.refs_4_), channel_id=1, source_target_pairs={{0,32},{32,0},{64,96},{96,64},{1,33},{33,1},{65,97},{97,65},{2,34}... | collective-permute-start | bytes 1179656 | tf_op jit(solution)/shard_map/ppermute | solution.py:216
  196.3 5.8 %collective-permute-start.8 = (bf16[4,384,128]{2,1,0:T(8,128)(2,1)S(1)}, bf16[4,384,128]{2,1,0:T(8,128)(2,1)S(1)}, u32[]{:S(2)}, u32[]{:S(2)}) collective-permute-start(bf16[4,384,128]{2,1,0:T(8,128)(2,1)S(1)} %pad_maximum_fusion.1.refs_4_), channel_id=1, source_target_pairs={{0,64},{32,96},{64,0},{96,32},{1,65},{33,97},{65,1},{97,33},{2,66}... | collective-permute-start | bytes 1179656 | tf_op jit(solution)/shard_map/ppermute | solution.py:216
  202.1 2.2 collective-permute-start.9
  204.3 0.7 copy.17.routes
  205.0 0.0 copy-done.15
  205.0 0.7 copy.18.route_weight
  205.8 2.7 %shard_map.155 = (bf16[128,512]{1,0:T(8,128)(2,1)}, bf16[128,512]{1,0:T(8,128)(2,1)}, bf16[4,128,256]{2,1,0:T(8,128)(2,1)}, bf16[4,128,256]{2,1,0:T(8,128)(2,1)}) custom-call(s32[128,4]{1,0:T(8,128)} %copy.17.routes, f32[128,4]{1,0:T(8,128)} %copy.18.route_weight), custom_call_target="tpu_custom_call" | custom-call | flops 10000000 | bytes 790528 | tf_op jit(solution)/shard_map/pallas_call | solution.py:46
  208.5 0.0 collective-permute-done.7.refs_5_
  208.5 7.8 %collective-permute-done.8.refs_6_ = bf16[4,384,128]{2,1,0:T(8,128)(2,1)S(1)} collective-permute-done((bf16[4,384,128]{2,1,0:T(8,128)(2,1)S(1)}, bf16[4,384,128]{2,1,0:T(8,128)(2,1)S(1)}, u32[]{:S(2)}, u32[]{:S(2)}) %collective-permute-start.8) | collective-permute-done | bytes 393248 | tf_op jit(solution)/shard_map/ppermute | solution.py:216
  216.3 6.3 %collective-permute-done.9.refs_7_ = bf16[4,384,128]{2,1,0:T(8,128)(2,1)} collective-permute-done((bf16[4,384,128]{2,1,0:T(8,128)(2,1)S(1)}, bf16[4,384,128]{2,1,0:T(8,128)(2,1)}, u32[]{:S(2)}, u32[]{:S(2)}) %collective-permute-start.9) | collective-permute-done | bytes 393248 | tf_op jit(solution)/shard_map/ppermute | solution.py:216
  222.7 4.5 %shard_map.159 = (bf16[1,256,2048]{2,1,0:T(8,128)(2,1)}, bf16[1,256,2048]{2,1,0:T(8,128)(2,1)}, bf16[1,256,2048]{2,1,0:T(8,128)(2,1)}, bf16[16,2048]{1,0:T(8,128...) custom-call(s32[1]{0:T(128)} %bitcast.3.index, bf16[48,2048]{1,0:T(8,128)(2,1)} %shard_map.156.shr, ...), custom_call_target="tpu_custom_call" | custom-call | flops 10000000 | bytes 6881284 | tf_op jit(solution)/shard_map/pallas_call | solution.py:46
  227.2 5.9 %shard_map.157.shared_hbm = f32[128,2048]{1,0:T(8,128)} custom-call(bf16[128,2048]{1,0:T(8,128)(2,1)} %get-tuple-element.28.normed, bf16[32,48,2048]{2,1,0:T(8,128)(2,1)} %bitcast.9), custom_call_target="tpu_custom_call" | custom-call | flops 805306368 | bytes 7864320 | tf_op jit(solution)/shard_map/pallas_call | solution.py:46
  233.1 0.0 all-to-all-done.2.returned
  233.1 1.2 copy-done.1
  234.4 2.0 shard_map.158
  (28 shorter events, 0.1 us)
Async XLA Ops:
  7.2 93.4 %all-gather.5.cloned.1.call-start = ((), (), s32[]{:S(2)}) async-start(), calls=%async_computation.3 | async-start | bytes 3342336 | tf_op jit(solution)/shard_map/all_gather | solution.py:262
  9.1 218.1 %all-gather.7.cloned.1.call-start = ((), (), s32[]{:S(2)}) async-start(), calls=%async_computation.4 | async-start | bytes 6488064 | tf_op jit(solution)/shard_map/all_gather | solution.py:279
  9.1 6.9 %collective-permute-start = (bf16[432,128]{1,0:T(8,128)(2,1)}, bf16[432,128]{1,0:T(8,128)(2,1)S(1)}, u32[]{:S(2)}, u32[]{:S(2)}) collective-permute-start(bf16[432,128]{1,0:T(8,128)(2,1)} %get-tuple-element.29), channel_id=1, source_target_pairs={{0,32},{32,0},{64,96},{96,64},{1,33},{33,1},{65,97},{97,65},{2,34}... | collective-permute-start | bytes 331784 | tf_op jit(solution)/shard_map/ppermute | solution.py:216
  16.9 9.7 %collective-permute-start.1 = (bf16[2,432,128]{2,1,0:T(8,128)(2,1)S(1)}, bf16[2,432,128]{2,1,0:T(8,128)(2,1)S(1)}, u32[]{:S(2)}, u32[]{:S(2)}) collective-permute-start(bf16[2,432,128]{2,1,0:T(8,128)(2,1)S(1)} %pad_maximum_fusion.2), channel_id=1, source_target_pairs={{0,64},{32,96},{64,0},{96,32},{1,65},{33,97},{65,1},{97,33},{2,66}... | collective-permute-start | bytes 663560 | tf_op jit(solution)/shard_map/ppermute | solution.py:216
  27.6 30.5 %copy-start.6 = (bf16[4,432,128]{2,1,0:T(8,128)(2,1)}, bf16[4,432,128]{2,1,0:T(8,128)(2,1)S(1)}, u32[]{:S(2)}) copy-start(bf16[4,432,128]{2,1,0:T(8,128)(2,1)S(1)} %pad_maximum_fusion.refs_0_) | copy-start | bytes 1327108
  27.6 14.9 %collective-permute-start.2 = (bf16[4,432,128]{2,1,0:T(8,128)(2,1)S(1)}, bf16[4,432,128]{2,1,0:T(8,128)(2,1)S(1)}, u32[]{:S(2)}, u32[]{:S(2)}) collective-permute-start(bf16[4,432,128]{2,1,0:T(8,128)(2,1)S(1)} %pad_maximum_fusion.refs_0_), channel_id=1, source_target_pairs={{0,128},{128,0},{256,384},{384,256},{1,129},{129,1},{257,385},{385... | collective-permute-start | bytes 1327112 | tf_op jit(solution)/shard_map/ppermute | solution.py:216
  31.1 20.6 %collective-permute-start.3 = (bf16[4,432,128]{2,1,0:T(8,128)(2,1)S(1)}, bf16[4,432,128]{2,1,0:T(8,128)(2,1)S(1)}, u32[]{:S(2)}, u32[]{:S(2)}) collective-permute-start(bf16[4,432,128]{2,1,0:T(8,128)(2,1)S(1)} %pad_maximum_fusion.refs_0_), channel_id=1, source_target_pairs={{0,256},{128,384},{256,0},{384,128},{1,257},{129,385},{257,1},{385... | collective-permute-start | bytes 1327112 | tf_op jit(solution)/shard_map/ppermute | solution.py:216
  35.9 22.2 %collective-permute-start.4 = (bf16[4,432,128]{2,1,0:T(8,128)(2,1)S(1)}, bf16[4,432,128]{2,1,0:T(8,128)(2,1)S(1)}, u32[]{:S(2)}, u32[]{:S(2)}) collective-permute-start(bf16[4,432,128]{2,1,0:T(8,128)(2,1)S(1)} %pad_maximum_fusion.refs_0_), channel_id=1, source_target_pairs={{0,384},{128,256},{256,128},{384,0},{1,385},{129,257},{257,129},{3... | collective-permute-start | bytes 1327112 | tf_op jit(solution)/shard_map/ppermute | solution.py:216
  42.5 15.6 %copy-start.7 = (bf16[4,432,128]{2,1,0:T(8,128)(2,1)}, bf16[4,432,128]{2,1,0:T(8,128)(2,1)S(1)}, u32[]{:S(2)}) copy-start(bf16[4,432,128]{2,1,0:T(8,128)(2,1)S(1)} %collective-permute-done.2.refs_1_) | copy-start | bytes 1327108
  51.7 6.4 %copy-start.8 = (bf16[4,432,128]{2,1,0:T(8,128)(2,1)}, bf16[4,432,128]{2,1,0:T(8,128)(2,1)S(1)}, u32[]{:S(2)}) copy-start(bf16[4,432,128]{2,1,0:T(8,128)(2,1)S(1)} %collective-permute-done.3.refs_2_) | copy-start | bytes 1327108
  58.1 0.7 copy-start.9
  148.5 1.5 copy-start
  150.0 4.2 %copy-start.11 = (bf16[384,128]{1,0:T(8,128)(2,1)S(1)}, bf16[384,128]{1,0:T(8,128)(2,1)}, u32[]{:S(2)}) copy-start(bf16[384,128]{1,0:T(8,128)(2,1)} %get-tuple-element.30) | copy-start | bytes 294916
  150.0 54.3 %copy-start.14 = (s32[128,4]{0,1:T(4,128)S(1)}, s32[128,4]{0,1:T(4,128)}, u32[]{:S(2)}) copy-start(s32[128,4]{0,1:T(4,128)} %param.18) | copy-start | bytes 6148
  150.0 55.1 %copy-start.15 = (f32[128,4]{0,1:T(4,128)S(1)}, f32[128,4]{0,1:T(4,128)}, u32[]{:S(2)}) copy-start(f32[128,4]{0,1:T(4,128)} %param.19) | copy-start | bytes 6148
  150.0 83.1 %all-to-all-start.2 = ((bf16[32,72,512]{2,1,0:T(8,128)(2,1)}), bf16[32,72,512]{2,1,0:T(8,128)(2,1)S(1)}, u32[]{:S(2)}, u32[]{:S(2)}) async-start(bf16[32,72,512]{2,1,0:T(8,128)(2,1)} %copy-done), calls=%async_computation.2 | async-start | bytes 4718592 | tf_op jit(solution)/shard_map/all_to_all | solution.py:305
  154.2 29.8 %collective-permute-start.5 = (bf16[384,128]{1,0:T(8,128)(2,1)S(1)}, bf16[384,128]{1,0:T(8,128)(2,1)S(1)}, u32[]{:S(2)}, u32[]{:S(2)}) collective-permute-start(bf16[384,128]{1,0:T(8,128)(2,1)S(1)} %copy-done.11), channel_id=1, source_target_pairs={{0,128},{128,0},{256,384},{384,256},{1,129},{129,1},{257,385},{385... | collective-permute-start | bytes 294920 | tf_op jit(solution)/shard_map/ppermute | solution.py:216
  184.0 9.7 %collective-permute-start.6 = (bf16[2,384,128]{2,1,0:T(8,128)(2,1)S(1)}, bf16[2,384,128]{2,1,0:T(8,128)(2,1)S(1)}, u32[]{:S(2)}, u32[]{:S(2)}) collective-permute-start(bf16[2,384,128]{2,1,0:T(8,128)(2,1)S(1)} %pad_maximum_fusion.3), channel_id=1, source_target_pairs={{0,256},{128,384},{256,0},{384,128},{1,257},{129,385},{257,1},{385... | collective-permute-start | bytes 589832 | tf_op jit(solution)/shard_map/ppermute | solution.py:216
  193.8 28.8 %copy-start.10 = (bf16[4,384,128]{2,1,0:T(8,128)(2,1)}, bf16[4,384,128]{2,1,0:T(8,128)(2,1)S(1)}, u32[]{:S(2)}) copy-start(bf16[4,384,128]{2,1,0:T(8,128)(2,1)S(1)} %pad_maximum_fusion.1.refs_4_) | copy-start | bytes 1179652
  193.8 14.7 %collective-permute-start.7 = (bf16[4,384,128]{2,1,0:T(8,128)(2,1)S(1)}, bf16[4,384,128]{2,1,0:T(8,128)(2,1)S(1)}, u32[]{:S(2)}, u32[]{:S(2)}) collective-permute-start(bf16[4,384,128]{2,1,0:T(8,128)(2,1)S(1)} %pad_maximum_fusion.1.refs_4_), channel_id=1, source_target_pairs={{0,32},{32,0},{64,96},{96,64},{1,33},{33,1},{65,97},{97,65},{2,34}... | collective-permute-start | bytes 1179656 | tf_op jit(solution)/shard_map/ppermute | solution.py:216
  196.3 20.1 %collective-permute-start.8 = (bf16[4,384,128]{2,1,0:T(8,128)(2,1)S(1)}, bf16[4,384,128]{2,1,0:T(8,128)(2,1)S(1)}, u32[]{:S(2)}, u32[]{:S(2)}) collective-permute-start(bf16[4,384,128]{2,1,0:T(8,128)(2,1)S(1)} %pad_maximum_fusion.1.refs_4_), channel_id=1, source_target_pairs={{0,64},{32,96},{64,0},{96,32},{1,65},{33,97},{65,1},{97,33},{2,66}... | collective-permute-start | bytes 1179656 | tf_op jit(solution)/shard_map/ppermute | solution.py:216
  202.1 20.5 %collective-permute-start.9 = (bf16[4,384,128]{2,1,0:T(8,128)(2,1)S(1)}, bf16[4,384,128]{2,1,0:T(8,128)(2,1)}, u32[]{:S(2)}, u32[]{:S(2)}) collective-permute-start(bf16[4,384,128]{2,1,0:T(8,128)(2,1)S(1)} %pad_maximum_fusion.1.refs_4_), channel_id=1, source_target_pairs={{0,96},{32,64},{64,32},{96,0},{1,97},{33,65},{65,33},{97,1},{2,98}... | collective-permute-start | bytes 1179656 | tf_op jit(solution)/shard_map/ppermute | solution.py:216
  208.5 14.1 %copy-start.12 = (bf16[4,384,128]{2,1,0:T(8,128)(2,1)}, bf16[4,384,128]{2,1,0:T(8,128)(2,1)S(1)}, u32[]{:S(2)}) copy-start(bf16[4,384,128]{2,1,0:T(8,128)(2,1)S(1)} %collective-permute-done.7.refs_5_) | copy-start | bytes 1179652
  216.3 6.3 %copy-start.13 = (bf16[4,384,128]{2,1,0:T(8,128)(2,1)}, bf16[4,384,128]{2,1,0:T(8,128)(2,1)S(1)}, u32[]{:S(2)}) copy-start(bf16[4,384,128]{2,1,0:T(8,128)(2,1)S(1)} %collective-permute-done.8.refs_6_) | copy-start | bytes 1179652
  227.2 5.9 %copy-start.2 = (bf16[4,128,256]{2,1,0:T(8,128)(2,1)S(1)}, bf16[4,128,256]{2,1,0:T(8,128)(2,1)}, u32[]{:S(2)}) copy-start(bf16[4,128,256]{2,1,0:T(8,128)(2,1)} %get-tuple-element.26.few_high) | copy-start | bytes 786436
  227.2 5.9 %copy-start.3 = (bf16[4,128,256]{2,1,0:T(8,128)(2,1)S(1)}, bf16[4,128,256]{2,1,0:T(8,128)(2,1)}, u32[]{:S(2)}) copy-start(bf16[4,128,256]{2,1,0:T(8,128)(2,1)} %get-tuple-element.27.few_low) | copy-start | bytes 786436
  227.2 5.9 %copy-start.4 = (bf16[128,512]{1,0:T(8,128)(2,1)S(1)}, bf16[128,512]{1,0:T(8,128)(2,1)}, u32[]{:S(2)}) copy-start(bf16[128,512]{1,0:T(8,128)(2,1)} %get-tuple-element.24.main_high) | copy-start | bytes 393220
  227.2 5.9 %copy-start.5 = (bf16[128,512]{1,0:T(8,128)(2,1)S(1)}, bf16[128,512]{1,0:T(8,128)(2,1)}, u32[]{:S(2)}) copy-start(bf16[128,512]{1,0:T(8,128)(2,1)} %get-tuple-element.25.main_low) | copy-start | bytes 393220
  233.1 1.2 copy-start.1
Sparse Core Ops, SparseCore 0:
  10.6 73.9 all-gather.4
  86.7 73.0 all-gather.6
